TPU v7x, 512 devices: a whole 4x4x16 slice. The times are simulated.
512 devices in a mesh: sp: 64 (over z, y), tp: 8 (over x, core).
Axes of the slice: x: 4, y: 4, z: 16, core: 2. Of those that a mesh axis runs over, the one named last changes fastest.
Arguments:
- tokens: bfloat16 [2, 16384, 2048], P(None, 'sp'), may hold values from -6 to 6
- key_weight: bfloat16 [2048, 2048], P(None, 'tp'), may hold values from -0.125 to 0.125
- value_weight: bfloat16 [2048, 2048], P(None, 'tp'), may hold values from -0.125 to 0.125
- cum_gate: float32 [2, 16384, 32], P(None, 'sp', 'tp'), may hold values from -1968.2 to 0, as said below
- new_input: bfloat16 [2, 2048], replicated, may hold values from -6 to 6
- new_query: bfloat16 [2, 2048], P(None, 'tp'), may hold values from -360 to 360
- new_gate: float32 [2, 32], P(None, 'tp'), may hold values from -1968.2 to 0
- out_weight: bfloat16 [2048, 2048], P('tp', 'sp'), may hold values from -0.75 to 0.75
Outputs:
- key_cache: bfloat16 [2, 64, 256, 2048], P(None, 'sp', None, 'tp')
- value_cache: bfloat16 [2, 64, 256, 2048], P(None, 'sp', None, 'tp')
- gate_cache: float32 [2, 64, 256, 32], P(None, 'sp', None, 'tp')
- mixed: bfloat16 [2, 2048], P(None, 'sp')
Inputs may be any that keep to these rules, and one draw needn't show every extreme that they name: For each sequence and head cum_gate does not rise along positions, and new_gate lies at or below the value at the last cached position.
All inputs are finite; a program needn't handle non-finite values.
Results may differ from a plain program's by a relative error of at most 0.015.
Values may be sent and summed in bfloat16 or wider, within the bound.
A program may use at most 64 MiB of HBM per device.

v0:
```python
import jax
import jax.numpy as jnp
from jax import lax
from jax.sharding import Mesh
from jax.sharding import PartitionSpec as P

SP = ("sp_0", "sp_1")


def side_by_side(arrays, axis, split_dim, concat_dim, along):
    widths = [a.shape[along] for a in arrays]
    both = jnp.concatenate(arrays, axis=along)
    out = lax.all_to_all(both, axis, split_axis=split_dim, concat_axis=concat_dim, tiled=True)
    return tuple(jnp.split(out, [sum(widths[:k]) for k in range(1, len(widths))], axis=along))


def split_up(x, dim, devices):
    shape = x.shape
    parts = x.reshape(*shape[:dim], devices, shape[dim] // devices, *shape[dim + 1 :])
    return jnp.moveaxis(parts, dim, 0)


def in_order(parts, dim):
    shape = list(parts.shape[1:])
    shape[dim] *= parts.shape[0]
    return jnp.moveaxis(parts, 0, dim).reshape(shape)


def turned_blocks(parts, axes, turns):
    inside = parts.shape[1:]
    out = parts.reshape(*(lax.axis_size(a) for a in axes), *inside)
    for k in turns:
        out = lax.all_to_all(out, axes[k], k, k, tiled=True)
    return out.reshape(-1, *inside)


def exchange_by_axis(x, axes, turns, split_dim, concat_dim):
    parts = split_up(x, split_dim, lax.axis_size(axes))
    return in_order(turned_blocks(parts, axes, turns), concat_dim)


def copy_for_each(x, axis):
    copies = jnp.broadcast_to(x, (lax.axis_size(axis), *x.shape))
    return lax.all_to_all(copies, axis, split_axis=0, concat_axis=0, tiled=True)


def all_in_one(x, axis):
    leaves = jax.tree.leaves(x)
    turns = sorted(range(len(leaves)), key=lambda k: -leaves[k].size)
    width = (1, *leaves[turns[0]].shape)[-1]
    lines = [
        jnp.pad(leaves[k].reshape(-1), (0, -leaves[k].size % width)).reshape(-1, width)
        for k in turns
    ]
    both, at, found = (copy_for_each(jnp.concatenate(lines), axis), 0, {})
    for k, line in zip(turns, lines):
        share = both[:, at : at + len(line)].reshape(len(both), -1)
        found[k] = share[:, : leaves[k].size].reshape(-1, *leaves[k].shape)
        at += len(line)
    numbers = iter(range(len(leaves)))
    return jax.tree.map(lambda _: found[next(numbers)], x)


def combined_pairwise(pieces, combine):
    while len(jax.tree.leaves(pieces)[0]) > 1:
        pieces = jax.vmap(combine)(
            *(jax.tree.map(lambda part: part[side::2], pieces) for side in (0, 1))
        )
    return jax.tree.map(lambda part: part[0], pieces)


def merged(x, axis, combine):
    pieces = all_in_one(x, axis)
    return combined_pairwise(pieces, combine)


def over_copies(x, axis):
    return copy_for_each(x, axis).astype(jnp.float32).sum(axis=0)


def combine_parts(first, second):
    highest = jnp.maximum(first[0], second[0])
    first_scale = jnp.exp(first[0] - highest)
    second_scale = jnp.exp(second[0] - highest)
    total = first[1] * first_scale + second[1] * second_scale
    numer = first[2] * first_scale[:, :, None] + second[2] * second_scale[:, :, None]
    return (highest, total, numer)


def body(tokens, key_weight, value_weight, cum_gate, new_input, new_query, new_gate, out_weight):
    local_width = key_weight.shape[1]
    parts = lax.axis_size(SP)
    seq_count, span, width = tokens.shape
    per_peer = span // parts
    flat_rows = tokens.reshape(seq_count * span, width)
    key_local = jnp.dot(flat_rows, key_weight, preferred_element_type=jnp.float32).astype(
        jnp.bfloat16
    )
    value_local = jnp.dot(flat_rows, value_weight, preferred_element_type=jnp.float32).astype(
        jnp.bfloat16
    )
    shaped = (seq_count, per_peer, parts, local_width)
    key_moved, value_moved = side_by_side(
        (key_local.reshape(shaped), value_local.reshape(shaped)), SP, 2, 1, 0
    )
    key_cache = key_moved.reshape(seq_count, 1, span, local_width)
    value_cache = value_moved.reshape(seq_count, 1, span, local_width)
    head_count = cum_gate.shape[2]
    gate_shaped = cum_gate.reshape(seq_count, per_peer, parts, head_count)
    gate_cache = exchange_by_axis(gate_shaped, SP, (0, 1), 2, 1).reshape(
        seq_count, 1, span, head_count
    )
    head_size = local_width // head_count
    score_scale = head_size ** (-0.5)
    key_now = jnp.dot(new_input, key_weight, preferred_element_type=jnp.float32).astype(
        jnp.bfloat16
    )
    value_now = jnp.dot(new_input, value_weight, preferred_element_type=jnp.float32).astype(
        jnp.bfloat16
    )
    key_now = key_now.reshape(seq_count, head_count, head_size)
    value_now = value_now.reshape(seq_count, head_count, head_size)
    query_heads = new_query.reshape(seq_count, head_count, head_size)
    key_heads = key_cache.reshape(seq_count, span, head_count, head_size)
    value_heads = value_cache.reshape(seq_count, span, head_count, head_size)
    scores = (
        jnp.einsum("nhd,nlhd->nhl", query_heads, key_heads, preferred_element_type=jnp.float32)
        * score_scale
    )
    scores = (
        scores
        + new_gate[:, :, None]
        - jnp.swapaxes(gate_cache.reshape(seq_count, span, head_count), 1, 2)
    )
    class_top = jnp.max(scores, axis=2)
    expo = jnp.exp(scores - class_top[:, :, None])
    class_total = jnp.sum(expo, axis=2)
    class_num = jnp.einsum(
        "nhl,nlhd->nhd", expo.astype(jnp.bfloat16), value_heads, preferred_element_type=jnp.float32
    )
    cached_top, cached_total, cached_num = merged(
        (class_top, class_total, class_num), SP, combine_parts
    )
    own_score = (
        jnp.einsum("nhd,nhd->nh", query_heads, key_now, preferred_element_type=jnp.float32)
        * score_scale
    )
    highest = jnp.maximum(cached_top, own_score)
    keep = jnp.exp(cached_top - highest)
    own_expo = jnp.exp(own_score - highest)
    totals = cached_total * keep + own_expo
    own_rounded = lax.optimization_barrier(own_expo.astype(jnp.bfloat16)).astype(jnp.float32)
    numerator = cached_num * keep[:, :, None] + own_rounded[:, :, None] * value_now.astype(
        jnp.float32
    )
    attended = (numerator / totals[:, :, None]).astype(jnp.bfloat16).reshape(seq_count, local_width)
    partial_value = jnp.dot(attended, out_weight, preferred_element_type=jnp.float32)
    partial_value = lax.optimization_barrier(partial_value.astype(jnp.bfloat16)).astype(jnp.float32)
    mixed = (
        over_copies(partial_value.astype(jnp.bfloat16), "tp")
        .astype(jnp.float32)
        .astype(jnp.bfloat16)
    )
    return (key_cache, value_cache, gate_cache, mixed)


def solution(mesh):
    torus = Mesh(mesh.devices.reshape(16, 4, mesh.shape["tp"]), ("sp_0", "sp_1", "tp"))
    in_specs = (
        P(None, SP, None),
        P(None, "tp"),
        P(None, "tp"),
        P(None, SP, "tp"),
        P(),
        P(None, "tp"),
        P(None, "tp"),
        P("tp", SP),
    )
    out_specs = (
        P(None, SP, None, "tp"),
        P(None, SP, None, "tp"),
        P(None, SP, None, "tp"),
        P(None, SP),
    )
    return jax.shard_map(body, mesh=torus, in_specs=in_specs, out_specs=out_specs, check_vma=False)
```

profile of v0, /device:TPU:1, one launch (start us, length us, event | category | flops | bytes accessed | tf_op | source)
XLA Modules:
  0.0 129.5 jit_solution(17730495870390405574)
XLA Ops:
  0.6 0.9 reshape_reshape.15
  1.6 0.2 reshape.102
  1.8 0.1 copy.177
  1.9 0.9 reshape.127
  2.8 15.7 %all-to-all-start.1 = ((f32[16,1,128]{2,1,0:T(1,128)}), f32[16,1,128]{2,1,0:T(1,128)S(1)}, u32[]{:S(2)}, u32[]{:S(2)}) async-start(f32[16,1,128]{2,1,0:T(1,128)} %reshape.127), calls=%async_computation.1 | async-start | bytes 16384 | tf_op jit(solution)/shard_map/all_to_all | solution.py:33
  18.5 1.9 %convolution_convert_fusion = bf16[512,256]{1,0:T(8,128)(2,1)S(1)} fusion(bf16[512,2048]{1,0:T(8,128)(2,1)S(1)} %bitcast.115, bf16[2048,256]{1,0:T(8,128)(2,1)} %param.10), kind=kOutput, calls=%fused_computation | convolution fusion | flops 537001984 | bytes 3407872 | tf_op jit(solution)/shard_map/dot_general | solution.py:99
  20.5 0.7 convolution_convert_fusion.1
  21.2 0.2 copy.126
  21.4 0.2 copy.125
  21.6 8.1 %all-to-all-done.1 = f32[16,1,128]{2,1,0:T(1,128)S(1)} async-done(((f32[16,1,128]{2,1,0:T(1,128)}), f32[16,1,128]{2,1,0:T(1,128)S(1)}, u32[]{:S(2)}, u32[]{:S(2)}) %all-to-all-start.1) | async-done | bytes 8224 | tf_op jit(solution)/shard_map/all_to_all | solution.py:33
  29.8 0.5 broadcast.39
  30.3 0.7 reduce.11
  30.9 0.3 reshape.128
  31.3 0.3 copy.131
  31.6 0.7 reshape.129
  32.3 4.2 %all-to-all-start.2 = ((f32[4,1,512]{2,1,0:T(1,128)}), f32[4,1,512]{2,1,0:T(1,128)S(1)}, u32[]{:S(2)}, u32[]{:S(2)}) async-start(f32[4,1,512]{2,1,0:T(1,128)} %reshape.129), calls=%async_computation.2 | async-start | bytes 16384 | tf_op jit(solution)/shard_map/all_to_all | solution.py:33
  36.5 1.1 pad_maximum_fusion
  37.6 3.0 %all-to-all-done.2 = f32[4,1,512]{2,1,0:T(1,128)S(1)} async-done(((f32[4,1,512]{2,1,0:T(1,128)}), f32[4,1,512]{2,1,0:T(1,128)S(1)}, u32[]{:S(2)}, u32[]{:S(2)}) %all-to-all-start.2) | async-done | bytes 8224 | tf_op jit(solution)/shard_map/all_to_all | solution.py:33
  40.7 4.8 %all-to-all-start = ((bf16[4,4,64,256]{3,1,0,2:T(4,128)(2,1)}), bf16[4,4,64,256]{3,1,0,2:T(4,128)(2,1)S(1)}, u32[]{:S(2)}, u32[]{:S(2)}) async-start(bf16[4,4,64,256]{3,1,0,2:T(4,128)(2,1)} %pad_maximum_fusion), calls=%async_computation | async-start | bytes 1048576 | tf_op jit(solution)/shard_map/all_to_all | solution.py:13
  45.6 0.7 reduce.12
  46.3 0.1 reshape.130
  46.4 0.3 copy.132
  46.7 0.2 reshape.103
  46.8 0.2 copy.133
  47.0 0.2 reshape_reshape_reshape.3
  47.2 26.3 %all-to-all-done = bf16[4,4,64,256]{3,1,0,2:T(4,128)(2,1)S(1)} async-done(((bf16[4,4,64,256]{3,1,0,2:T(4,128)(2,1)}), bf16[4,4,64,256]{3,1,0,2:T(4,128)(2,1)S(1)}, u32[]{:S(2)}, u32[]{:S(2)}) %all-to-all-start) | async-done | bytes 524320 | tf_op jit(solution)/shard_map/all_to_all | solution.py:13
  73.5 0.2 fusion.29
  73.8 1.1 reshape_reshape.17
  74.9 1.3 fusion.9
  76.2 0.2 fusion.27
  76.4 0.2 fusion.15
  76.8 1.1 reshape_reshape.18
  77.9 1.2 fusion.7
  79.1 0.9 reshape.131
  80.0 8.9 %all-to-all-start.3 = ((f32[64,1,640]{2,1,0:T(1,128)}), f32[64,1,640]{2,1,0:T(1,128)S(1)}, u32[]{:S(2)}, u32[]{:S(2)}) async-start(f32[64,1,640]{2,1,0:T(1,128)} %reshape.131), calls=%async_computation.3 | async-start | bytes 327680 | tf_op jit(solution)/shard_map/all_to_all | solution.py:44
  89.0 1.5 %convolution_convert_fusion.3 = bf16[2,256]{1,0:T(2,128)(2,1)S(1)} fusion(bf16[2,2048]{1,0:T(2,128)(2,1)S(1)} %copy-done.2, bf16[2048,256]{1,0:T(8,128)(2,1)} %param.9), kind=kOutput, calls=%fused_computation.8 | convolution fusion | flops 2097664 | bytes 1057792 | tf_op jit(solution)/shard_map/dot_general | solution.py:115
  90.7 13.9 %all-to-all-done.3 = f32[64,1,640]{2,1,0:T(1,128)S(1)} async-done(((f32[64,1,640]{2,1,0:T(1,128)}), f32[64,1,640]{2,1,0:T(1,128)S(1)}, u32[]{:S(2)}, u32[]{:S(2)}) %all-to-all-start.3) | async-done | bytes 163872 | tf_op jit(solution)/shard_map/all_to_all | solution.py:44
  104.6 1.7 %reduce.13 = f32[64,640]{1,0:T(8,128)} reduce(f32[64,1,640]{2,1,0:T(1,128)S(1)} %all-to-all-done.3, f32[]{:T(128)} %broadcast.39), dimensions={1}, to_apply=%all_to_all.28.reduce_sub_computation | reduce | bytes 327684 | tf_op jit(solution)/shard_map/all_to_all | solution.py:44
  106.3 1.0 reshape.132
  107.4 0.1 slice.161
  107.6 0.1 slice.160
  107.8 0.1 slice.135
  107.9 0.1 slice.136
  108.0 0.1 slice.163
  108.1 0.1 slice.162
  108.3 0.1 slice.139
  108.4 0.1 slice.140
  108.7 0.1 slice.143
  109.7 0.7 slice.172
  110.4 0.2 fusion.23
  110.9 0.1 copy.139
  111.0 0.1 copy.138
  111.9 1.2 multiply_add_fusion
  113.1 0.1 multiply_add_fusion.1
  113.8 1.6 %fusion.6 = bf16[2,32]{1,0:T(2,128)(2,1)S(1)} fusion(bf16[256,32]{0,1:T(8,128)(2,1)S(1)} %copy-done.3, f32[2,256]{1,0:T(2,128)S(1)} %div.12, f32[2,256]{1,0:T(2,128)S(1)} %mul.203, bf16[2,2048]{1,0:T(2,128)(2,1)S(1)} %copy-done.2, bf16[2048,256]{1,0:T(8,128)(2,1)} %param.10, f32[2,256]{1,0:T(2,128)S(1)} %squeeze.9, f32[2,256]{1,0:T(2,128)S(1)} %mul.200), kind=kOutput, calls=%fused_computation.10 | convolution fusion | flops 2133568 | bytes 1081472 | tf_op jit(solution)/shard_map/dot_general | solution.py:157
  115.4 0.6 broadcast_in_dim.5
  116.0 8.3 %all-to-all-start.4 = ((bf16[8,2,32]{2,1,0:T(2,128)(2,1)}), bf16[8,2,32]{2,1,0:T(2,128)(2,1)S(1)}, u32[]{:S(2)}, u32[]{:S(2)}) async-start(bf16[8,2,32]{2,1,0:T(2,128)(2,1)} %broadcast_in_dim.5), calls=%async_computation.4 | async-start | bytes 8192 | tf_op jit(solution)/shard_map/all_to_all | solution.py:44
  124.4 0.8 reshape_reshape.16
  125.1 0.2 copy.127
  125.3 0.2 copy.128
  125.5 0.7 copy.150
  126.3 0.7 copy.151
  127.0 1.9 %all-to-all-done.4 = bf16[8,2,32]{2,1,0:T(2,128)(2,1)S(1)} async-done(((bf16[8,2,32]{2,1,0:T(2,128)(2,1)}), bf16[8,2,32]{2,1,0:T(2,128)(2,1)S(1)}, u32[]{:S(2)}, u32[]{:S(2)}) %all-to-all-start.4) | async-done | bytes 1056 | tf_op jit(solution)/shard_map/all_to_all | solution.py:44
  129.0 0.5 reduce_sum.22
  (65 shorter events, 3.8 us)
Async XLA Ops:
  0.6 17.9 %copy-start = (bf16[2,256,2048]{2,1,0:T(8,128)(2,1)S(1)}, bf16[2,256,2048]{2,1,0:T(8,128)(2,1)}, u32[]{:S(2)}) copy-start(bf16[2,256,2048]{2,1,0:T(8,128)(2,1)} %param.8) | copy-start | bytes 6291460
  1.9 18.6 %copy-start.1 = (bf16[2048,256]{1,0:T(8,128)(2,1)S(1)}, bf16[2048,256]{1,0:T(8,128)(2,1)}, u32[]{:S(2)}) copy-start(bf16[2048,256]{1,0:T(8,128)(2,1)} %param.9) | copy-start | bytes 3145732
  2.8 27.0 %all-to-all-start.1 = ((f32[16,1,128]{2,1,0:T(1,128)}), f32[16,1,128]{2,1,0:T(1,128)S(1)}, u32[]{:S(2)}, u32[]{:S(2)}) async-start(f32[16,1,128]{2,1,0:T(1,128)} %reshape.127), calls=%async_computation.1 | async-start | bytes 16384 | tf_op jit(solution)/shard_map/all_to_all | solution.py:33
  21.2 24.4 %copy-start.4 = (bf16[2,256]{1,0:T(2,128)(2,1)S(1)}, bf16[2,256]{1,0:T(2,128)(2,1)}, u32[]{:S(2)}) copy-start(bf16[2,256]{1,0:T(2,128)(2,1)} %param.13) | copy-start | bytes 3076
  32.3 8.4 %all-to-all-start.2 = ((f32[4,1,512]{2,1,0:T(1,128)}), f32[4,1,512]{2,1,0:T(1,128)S(1)}, u32[]{:S(2)}, u32[]{:S(2)}) async-start(f32[4,1,512]{2,1,0:T(1,128)} %reshape.129), calls=%async_computation.2 | async-start | bytes 16384 | tf_op jit(solution)/shard_map/all_to_all | solution.py:33
  40.7 32.8 %all-to-all-start = ((bf16[4,4,64,256]{3,1,0,2:T(4,128)(2,1)}), bf16[4,4,64,256]{3,1,0,2:T(4,128)(2,1)S(1)}, u32[]{:S(2)}, u32[]{:S(2)}) async-start(bf16[4,4,64,256]{3,1,0,2:T(4,128)(2,1)} %pad_maximum_fusion), calls=%async_computation | async-start | bytes 1048576 | tf_op jit(solution)/shard_map/all_to_all | solution.py:13
  46.4 29.8 %copy-start.5 = (f32[2,4]{1,0:T(2,128)S(1)}, f32[2,4]{1,0:T(2,128)}, u32[]{:S(2)}) copy-start(f32[2,4]{1,0:T(2,128)} %param.14) | copy-start | bytes 100
  74.9 14.1 %copy-start.2 = (bf16[2,2048]{1,0:T(2,128)(2,1)S(1)}, bf16[2,2048]{1,0:T(2,128)(2,1)}, u32[]{:S(2)}) copy-start(bf16[2,2048]{1,0:T(2,128)(2,1)} %param.12) | copy-start | bytes 24580
  80.0 24.5 %all-to-all-start.3 = ((f32[64,1,640]{2,1,0:T(1,128)}), f32[64,1,640]{2,1,0:T(1,128)S(1)}, u32[]{:S(2)}, u32[]{:S(2)}) async-start(f32[64,1,640]{2,1,0:T(1,128)} %reshape.131), calls=%async_computation.3 | async-start | bytes 327680 | tf_op jit(solution)/shard_map/all_to_all | solution.py:44
  89.0 24.8 %copy-start.3 = (bf16[256,32]{0,1:T(8,128)(2,1)S(1)}, bf16[256,32]{0,1:T(8,128)(2,1)}, u32[]{:S(2)}) copy-start(bf16[256,32]{0,1:T(8,128)(2,1)} %param.15) | copy-start | bytes 49156
  116.0 12.9 %all-to-all-start.4 = ((bf16[8,2,32]{2,1,0:T(2,128)(2,1)}), bf16[8,2,32]{2,1,0:T(2,128)(2,1)S(1)}, u32[]{:S(2)}, u32[]{:S(2)}) async-start(bf16[8,2,32]{2,1,0:T(2,128)(2,1)} %broadcast_in_dim.5), calls=%async_computation.4 | async-start | bytes 8192 | tf_op jit(solution)/shard_map/all_to_all | solution.py:44
where the time goes:
time: 130 us; the launch traced here: 129 us
  waiting for transfers between devices  53.4 us (41%)
  starting transfers between devices  42 us (32%)
  local copies, waits for them, and re-layouts  17.9 us (14%)
  matrix products  8.2 us (6%)
  other arithmetic  7.03 us (5%)
    all_to_all x1, waiting for transfers between devices, side_by_side(): lax.all_to_all(both, axis, split_axis=split_dim, concat_axis=concat_dim,...  26.3 us
    all_to_all x2, starting transfers between devices, turned_blocks(): out = lax.all_to_all(out, axes[k], k, k, tiled=True)  19.9 us
    all_to_all x2, starting transfers between devices, copy_for_each(): return lax.all_to_all(copies, axis, split_axis=0, concat_axis=0, tiled=True)  17.2 us
    all_to_all x2, waiting for transfers between devices, copy_for_each(): return lax.all_to_all(copies, axis, split_axis=0, concat_axis=0, tiled=True)  15.9 us
    all_to_all x2, waiting for transfers between devices, turned_blocks(): out = lax.all_to_all(out, axes[k], k, k, tiled=True)  11.2 us
    unnamed x22, local copies, waits for them, and re-layouts  5.6 us
    all_to_all x1, starting transfers between devices, side_by_side(): lax.all_to_all(both, axis, split_axis=split_dim, concat_axis=concat_dim,...  4.84 us
  transfers between devices with their start and end apart: 5, of which 5 were waited for; matrix products, arithmetic and copies ran while one was open for 8% of the time, Pallas kernels for 0%

commit v1 on v0

v1 whole, which is shorter than its diff:
```python
import jax
import jax.numpy as jnp
from jax import lax
from jax.experimental import pallas as pl
from jax.experimental.pallas import tpu as pltpu
from jax.sharding import Mesh
from jax.sharding import PartitionSpec as P

MESH = pl.DeviceIdType.MESH
F32 = jnp.float32
BF16 = jnp.bfloat16
NZ, NY, NX, NC = 16, 4, 4, 2
HIGH = lax.Precision.HIGHEST

ORDER = (1, 2, 3, 4, 8, 7, 6, 5)


def slots_of(d):
    if d == 0:
        return 0, 1
    if d == NZ // 2:
        return NZ - 1, 1
    return 2 * d - 1, 2


def iota(shape, dim):
    return lax.broadcasted_iota(jnp.int32, shape, dim)


def nt_dot(a, b, precision=None):
    return lax.dot_general(
        a, b, (((1,), (1,)), ((), ())), precision=precision, preferred_element_type=F32
    )


def fold_heads(wide):
    half = wide[:, :128] + wide[:, 128:]
    return half + pltpu.roll(half, 64, 1)


def merge(parts):
    tops = [p[:, 65:66] for p in parts]
    top = tops[0]
    for t in tops[1:]:
        top = jnp.maximum(top, t)
    total = None
    for p, t in zip(parts, tops):
        term = p * jnp.exp(t - top)
        total = term if total is None else total + term
    lane = iota(total.shape, 1)
    return jnp.where(lane == 65, top, total)


def kernel(
    tok_hbm, wk_hbm, wv_hbm, gate_ref, new_in_ref, query_ref, new_gate_ref, ow_ref,
    k_out, v_out, g_out, m_out,
    tok, wk, wv, part, sent, zbuf, tbuf, g8, pg, zg, yg, ap, ay, azs, az, afs, af, tps, tpr, kv_loc,
    sem_in, d_sem, zs_sem, ys_sem, xs_sem, cs_sem, zr_sem, yr_sem, xr_sem, cr_sem,
    gzs_sem, gzr_sem, gys_sem, gyr_sem, a_send, a_recv,
):
    z, y = lax.axis_index("z"), lax.axis_index("y")
    x, c = lax.axis_index("x"), lax.axis_index("c")
    me = x * NC + c

    def zat(d):
        return lax.rem(z + (d + NZ), NZ)

    def yat(d):
        return lax.rem(y + d, NY)

    def xat(d):
        return lax.rem(x + d, NX)

    def remote(src, dst, ssem, rsem, **dev):
        return pltpu.make_async_remote_copy(
            src_ref=src, dst_ref=dst, send_sem=ssem, recv_sem=rsem,
            device_id=dev, device_id_type=MESH,
        )

    def wait_bytes(ref, sem):
        pltpu.make_async_copy(ref, ref, sem).wait()

    def signal(sem, **dev):
        pl.semaphore_signal(sem, inc=1, device_id=dev, device_id_type=MESH)

    barrier = pltpu.get_barrier_semaphore()
    cols = pl.ds(pl.multiple_of(me * 256, 256), 256)
    load_part = pltpu.make_async_copy(tok_hbm.at[:, :, cols], part, sem_in.at[0])
    load_tok = pltpu.make_async_copy(tok_hbm, tok, sem_in.at[1])
    load_wk = pltpu.make_async_copy(wk_hbm, wk, sem_in.at[2])
    load_wv = pltpu.make_async_copy(wv_hbm, wv, sem_in.at[3])
    load_part.start()
    for dy in range(1, NY):
        signal(barrier, y=yat(dy))
    for dx in range(NX):
        for dc in range(NC):
            if dx or dc:
                signal(barrier, x=xat(dx), c=lax.rem(c + dc, NC))
    for dz in (1, -1):
        signal(barrier, z=zat(dz))
    load_wk.start()
    load_tok.start()
    load_wv.start()

    o, i = iota((512, 512), 0), iota((512, 512), 1)
    perm = (i == ((o & 4) << 6) + ((o & 3) << 6) + (o >> 3)).astype(F32).astype(BF16)
    load_part.wait()
    moved = jnp.dot(perm, part[...].reshape(512, 256), preferred_element_type=F32)
    sent[...] = moved.reshape(NZ, NY, 8, 256).astype(BF16)

    g8[0:4, :] = gate_ref[0]
    g8[4:8, :] = gate_ref[1]
    gates = g8[...]
    lanes, rows = iota((128, 256), 1), iota((128, 256), 0)
    spread = jnp.concatenate(
        [jnp.broadcast_to(gates[k : k + 1, :], (16, 256)) for k in range(8)], axis=0
    )
    same = ((lanes & 3) == ((rows >> 2) & 3)) & ((lanes >> 6) == (rows & 3))
    spread = jnp.where(same, spread, 0.0)
    pick = ((iota((16, 256), 1) >> 2) & 15) == iota((16, 256), 0)
    gate_rows = nt_dot(pick.astype(F32), spread, HIGH)
    for k in range(NZ):
        pg[k] = gate_rows[k : k + 1, :]

    def send_z(d):
        for sign in (1, -1) if d < NZ // 2 else (1,):
            first, count = slots_of(d)
            slot = first if sign < 0 or count == 1 else first + 1
            remote(
                sent.at[zat(sign * d)], zbuf.at[slot], zs_sem, zr_sem.at[d], z=zat(sign * d)
            ).start()
            remote(pg.at[zat(sign * d)], zg.at[z], gzs_sem, gzr_sem, z=zat(sign * d)).start()

    def slots(d):
        first, count = slots_of(d)
        return pl.ds(first, count)

    def y_forward(d):
        if d:
            wait_bytes(zbuf.at[slots(d)], zr_sem.at[d])
        for dy in range(1, NY):
            remote(
                zbuf.at[slots(d), yat(dy)], tbuf.at[me, slots(d), y], ys_sem, yr_sem.at[d],
                y=yat(dy),
            ).start()
        tbuf[me, slots(d), y] = zbuf[slots(d), y]

    def x_forward(d):
        wait_bytes(zbuf.at[slots(d), pl.ds(0, 3)], yr_sem.at[d])
        here = tbuf.at[me, slots(d)]
        for dx in range(1, NX):
            remote(here, here, xs_sem, xr_sem.at[d], x=xat(dx)).start()
        remote(here, here, cs_sem, cr_sem.at[d], c=1 - c).start()

    def c_forward(d):
        wait_bytes(tbuf.at[pl.ds(0, 3), slots(d)], xr_sem.at[d])
        for dx in range(1, NX):
            there = tbuf.at[xat(dx) * NC + c, slots(d)]
            remote(there, there, cs_sem, cr_sem.at[d], c=1 - c).start()

    def finish(ds):
        for d in ds:
            wait_bytes(tbuf.at[pl.ds(0, 4), slots(d)], cr_sem.at[d])
        first = min(slots_of(d)[0] for d in ds)
        count = sum(slots_of(d)[1] for d in ds)
        for w, out in ((wk, k_out), (wv, v_out)):
            acc = None
            for f in range(8):
                lhs = tbuf[f, first : first + count].reshape(count * NY, 8, 256)
                lhs = lhs.astype(F32).reshape(count * 32, 256).astype(BF16)
                term = jnp.dot(
                    lhs, w[f * 256 : (f + 1) * 256, :], preferred_element_type=F32
                )
                acc = term if acc is None else acc + term
            acc = acc.reshape(count * 2, 2, 8, 256)
            even, odd = acc[:, 0], acc[:, 1]
            low = iota(even.shape, 1) < 4
            for b, (a0, a1) in enumerate(
                ((even, pltpu.roll(odd, 4, 1)), (pltpu.roll(even, 4, 1), odd))
            ):
                block = jnp.where(low, a0, a1).reshape(count, 16, 256).astype(BF16)
                for k in range(count):
                    slot = first + k
                    rel = 0 if slot == 0 else 8 if slot == NZ - 1 else (
                        (slot + 1) // 2 if slot % 2 else -(slot // 2)
                    )
                    at = pl.multiple_of(zat(rel) * 16, 16)
                    out[b, pl.ds(at, 16), :] = block[k]

    pl.semaphore_wait(barrier, 3 + 7 + 2)
    for s in (1, -1):
        signal(d_sem.at[0], z=zat(s))
    send_z(1)
    zbuf[0] = sent[z]
    zg[z] = pg[z]
    y_forward(0)
    pl.semaphore_wait(d_sem.at[0], 2)
    for s in (2, -2):
        signal(d_sem.at[1], z=zat(s))
    send_z(2)

    head_of_row = iota((8, 256), 0) & 3
    mine = (iota((8, 256), 1) >> 6) == head_of_row
    second = iota((8, 256), 0) >= 4

    def by_row(two):
        return jnp.where(
            second, jnp.broadcast_to(two[1:2, :], (8, 256)), jnp.broadcast_to(two[0:1, :], (8, 256))
        )

    query = jnp.where(mine, by_row(query_ref[...].astype(F32)), 0.0)
    query_b = query.astype(BF16)
    load_wk.wait()
    load_tok.wait()
    new_in = new_in_ref[...]
    key_now = jnp.dot(new_in, wk[...], preferred_element_type=F32).astype(BF16).astype(F32)
    local = tok[...].reshape(512, 2048)
    kv_loc[...] = jnp.dot(local, wk[...], preferred_element_type=F32).astype(BF16)
    pl.semaphore_wait(d_sem.at[1], 2)
    for s in (4, -4):
        signal(d_sem.at[2], z=zat(s))
    send_z(3)
    send_z(4)
    y_forward(1)
    raw = jnp.where(
        second, nt_dot(query_b, kv_loc[256:, :]), nt_dot(query_b, kv_loc[:256, :])
    )
    ng = new_gate_ref[...]
    ng = jnp.where(
        iota((8, 4), 0) >= 4,
        jnp.broadcast_to(ng[1:2, :], (8, 4)),
        jnp.broadcast_to(ng[0:1, :], (8, 4)),
    )
    ng = jnp.sum(
        jnp.where((iota((8, 4), 0) & 3) == iota((8, 4), 1), ng, 0.0), axis=1, keepdims=True
    )
    scores = raw * 0.125 + ng - g8[...]
    top = jnp.max(scores, axis=1, keepdims=True)
    expo = jnp.exp(scores - top)
    total = jnp.sum(expo, axis=1, keepdims=True)
    expo_b = expo.astype(BF16)
    load_wv.wait()
    value_now = jnp.dot(new_in, wv[...], preferred_element_type=F32).astype(BF16).astype(F32)
    kv_loc[...] = jnp.dot(local, wv[...], preferred_element_type=F32).astype(BF16)
    x_forward(0)
    num = jnp.where(
        second,
        jnp.dot(expo_b, kv_loc[256:, :], preferred_element_type=F32),
        jnp.dot(expo_b, kv_loc[:256, :], preferred_element_type=F32),
    )
    num = fold_heads(jnp.where(mine, num, 0.0))
    lane = iota((8, 128), 1)
    packed = jnp.where(
        lane < 64, num, jnp.where(lane == 64, total, jnp.where(lane == 65, top, 0.0))
    )
    for k in range(NY):
        ap[k] = packed[2 * k : 2 * k + 2, :]
    for dy in range(1, NY):
        remote(ap.at[yat(dy)], ay.at[y], a_send.at[0], a_recv.at[0], y=yat(dy)).start()
    ay[y] = ap[y]
    y_forward(2)
    pl.semaphore_wait(d_sem.at[2], 2)
    send_z(8)
    send_z(7)
    x_forward(1)
    wait_bytes(ay.at[pl.ds(0, 3)], a_recv.at[0])
    merged = merge([ay[k] for k in range(NY)])
    azs[...] = merged
    az[z] = merged
    for d in range(1, NZ):
        remote(azs, az.at[z], a_send.at[1], a_recv.at[1], z=zat(d)).start()
    send_z(6)
    send_z(5)

    y_forward(3)
    c_forward(0)
    x_forward(2)
    y_forward(4)
    c_forward(1)
    x_forward(3)
    c_forward(2)
    x_forward(4)
    c_forward(3)
    c_forward(4)
    finish((0, 1, 2, 3, 4))
    y_forward(8)
    y_forward(7)
    x_forward(8)
    wait_bytes(az.at[pl.ds(0, 15)], a_recv.at[1])
    merged = merge([az[k] for k in range(NZ)])
    afs[...] = merged
    af[y] = merged
    for dy in range(1, NY):
        remote(afs, af.at[y], a_send.at[2], a_recv.at[2], y=yat(dy)).start()
    y_forward(6)
    x_forward(7)
    y_forward(5)
    wait_bytes(zg.at[pl.ds(0, 15)], gzr_sem)
    for dy in range(1, NY):
        remote(zg, yg.at[y], gys_sem, gyr_sem, y=yat(dy)).start()
    for k in range(NZ):
        yg[y, k] = zg[k]
    c_forward(8)
    x_forward(6)
    wait_bytes(af.at[pl.ds(0, 3)], a_recv.at[2])
    cached = jnp.concatenate([af[k] for k in range(NY)], axis=0)
    own = jnp.sum(query * by_row(key_now), axis=1, keepdims=True) * 0.125
    cached_top, cached_total = cached[:, 65:66], cached[:, 64:65]
    cached_num = jnp.where(lane < 64, cached, pltpu.roll(cached, 64, 1))
    highest = jnp.maximum(cached_top, own)
    keep = jnp.exp(cached_top - highest)
    own_expo = jnp.exp(own - highest)
    totals = cached_total * keep + own_expo
    value_rows = fold_heads(jnp.where(mine, by_row(value_now), 0.0))
    numer = cached_num * keep + own_expo.astype(BF16).astype(F32) * value_rows
    attended = (numer / totals).astype(BF16).astype(F32)
    attended = jnp.where(mine, jnp.concatenate([attended, attended], axis=1), 0.0).astype(BF16)
    piece = nt_dot(attended, ow_ref[...])
    piece = jnp.concatenate(
        [jnp.sum(piece[0:4], axis=0, keepdims=True), jnp.sum(piece[4:8], axis=0, keepdims=True)],
        axis=0,
    )
    piece = piece.astype(BF16).astype(F32)
    tps[...] = jnp.concatenate([piece] * 4, axis=1)
    tpr[me] = tps[...]
    for dx in range(NX):
        for dc in range(NC):
            if dx or dc:
                remote(
                    tps, tpr.at[me], a_send.at[3], a_recv.at[3],
                    x=xat(dx), c=lax.rem(c + dc, NC),
                ).start()
    x_forward(5)
    c_forward(7)
    c_forward(6)
    wait_bytes(yg.at[pl.ds(0, 3)], gyr_sem)
    field = (iota((16, 128), 1) >> 2) & 3
    gathered = jnp.zeros((16, 128), F32)
    for k in range(NY):
        rows16 = jnp.concatenate([yg[k, i] for i in range(NZ)], axis=0)
        shift = lax.rem(4 * (k - y) + 128, 128)
        gathered += pltpu.roll(jnp.where(field == y, rows16, 0.0), shift, 1)
    spread = jnp.concatenate(
        [jnp.broadcast_to(gathered[k : k + 1, :], (16, 128)) for k in range(NZ)], axis=0
    )
    same = (iota((256, 128), 0) & 15) == (iota((256, 128), 1) & 15)
    spread = jnp.where(same, spread, 0.0)
    pick = (iota((8, 128), 1) >> 4) == iota((8, 128), 0)
    gate_cols = nt_dot(pick.astype(F32), spread, HIGH)
    g_out[0] = gate_cols[0:4]
    g_out[1] = gate_cols[4:8]
    wait_bytes(tpr.at[pl.ds(0, 7)], a_recv.at[3])
    mixed = tpr[0]
    for k in range(1, NX * NC):
        mixed += tpr[k]
    m_out[...] = mixed[:, :32].astype(BF16)
    c_forward(5)
    finish((5, 6, 7, 8))
    wait_bytes(zbuf.at[pl.ds(0, 15)], zs_sem)
    wait_bytes(zbuf.at[pl.ds(0, 12)], ys_sem)
    wait_bytes(tbuf.at[pl.ds(0, 3)], xs_sem)
    wait_bytes(tbuf.at[pl.ds(0, 4)], cs_sem)
    wait_bytes(zg.at[pl.ds(0, 15)], gzs_sem)
    wait_bytes(yg.at[pl.ds(0, 3)], gys_sem)
    wait_bytes(ap.at[pl.ds(0, 3)], a_send.at[0])
    wait_bytes(az.at[pl.ds(0, 15)], a_send.at[1])
    wait_bytes(af.at[pl.ds(0, 3)], a_send.at[2])
    wait_bytes(tpr.at[pl.ds(0, 7)], a_send.at[3])


def body(tokens, key_weight, value_weight, cum_gate, new_input, new_query, new_gate, out_weight):
    vmem = pl.BlockSpec(memory_space=pltpu.VMEM)
    hbm = pl.BlockSpec(memory_space=pl.ANY)
    dma, regular = pltpu.SemaphoreType.DMA, pltpu.SemaphoreType.REGULAR
    keys, values, gates, mixed = pl.pallas_call(
        kernel,
        out_shape=(
            jax.ShapeDtypeStruct((2, 256, 256), BF16),
            jax.ShapeDtypeStruct((2, 256, 256), BF16),
            jax.ShapeDtypeStruct((2, 4, 256), F32),
            jax.ShapeDtypeStruct((2, 32), BF16),
        ),
        in_specs=[hbm, hbm, hbm, vmem, vmem, vmem, vmem, vmem],
        out_specs=(vmem, vmem, vmem, vmem),
        scratch_shapes=[
            pltpu.VMEM((2, 256, 2048), BF16),
            pltpu.VMEM((2048, 256), BF16),
            pltpu.VMEM((2048, 256), BF16),
            pltpu.VMEM((2, 256, 256), BF16),
            pltpu.VMEM((NZ, NY, 8, 256), BF16),
            pltpu.VMEM((NZ, NY, 8, 256), BF16),
            pltpu.VMEM((8, NZ, NY, 8, 256), BF16),
            pltpu.VMEM((8, 256), F32),
            pltpu.VMEM((NZ, 1, 128), F32),
            pltpu.VMEM((NZ, 1, 128), F32),
            pltpu.VMEM((NY, NZ, 1, 128), F32),
            pltpu.VMEM((NY, 2, 128), F32),
            pltpu.VMEM((NY, 2, 128), F32),
            pltpu.VMEM((2, 128), F32),
            pltpu.VMEM((NZ, 2, 128), F32),
            pltpu.VMEM((2, 128), F32),
            pltpu.VMEM((NY, 2, 128), F32),
            pltpu.VMEM((2, 128), F32),
            pltpu.VMEM((8, 2, 128), F32),
            pltpu.VMEM((512, 256), BF16),
            dma((4,)),
            regular((3,)),
            dma, dma, dma, dma,
            dma((9,)), dma((9,)), dma((9,)), dma((9,)),
            dma, dma, dma, dma,
            dma((4,)), dma((4,)),
        ],
        compiler_params=pltpu.CompilerParams(collective_id=0, has_side_effects=True),
    )(
        tokens, key_weight, value_weight, jnp.swapaxes(cum_gate, 1, 2), new_input, new_query,
        new_gate, out_weight.T,
    )
    return (
        keys.reshape(2, 1, 256, 256),
        values.reshape(2, 1, 256, 256),
        jnp.swapaxes(gates, 1, 2).reshape(2, 1, 256, 4),
        mixed,
    )


def solution(mesh):
    torus = Mesh(mesh.devices.reshape(NZ, NY, NX, NC), ("z", "y", "x", "c"))
    sp, tp = ("z", "y"), ("x", "c")
    return jax.shard_map(
        body,
        mesh=torus,
        in_specs=(
            P(None, sp, None), P(None, tp), P(None, tp), P(None, sp, tp), P(), P(None, tp),
            P(None, tp), P(tp, sp),
        ),
        out_specs=(P(None, sp, None, tp), P(None, sp, None, tp), P(None, sp, None, tp), P(None, sp)),
        check_vma=False,
    )
```

time: 130 us -> 55.2 us (0.42)
  waiting for transfers between devices: 53.4 us -> 0 us
  Pallas kernels: 0 us -> 48.4 us
  starting transfers between devices: 42 us -> 0 us
  local copies, waits for them, and re-layouts: 17.9 us -> 5.81 us
  matrix products: 8.2 us -> 0 us
  other arithmetic: 7.03 us -> 0 us
    all_to_all x5 -> x0, waiting for transfers between devices: 53.4 us -> none  [the longest x1 26.3 us: side_by_side(): lax.all_to_all(both, axis, split_axis=split_dim, concat_axis=concat_dim,...]
    pallas_call x0 -> x1, Pallas kernels: none -> 48.4 us  [body(): pl.pallas_call(kernel, out_shape=(jax.ShapeDtypeStruct((2, 256, 256), BF1...]
    all_to_all x5 -> x0, starting transfers between devices: 42 us -> none  [the longest x2 19.9 us: turned_blocks(): out = lax.all_to_all(out, axes[k], k, k, tiled=True)]
    dot_general x6 -> x0, matrix products: 8.2 us -> none  [the longest x1 1.93 us: body(): jnp.dot(flat_rows, value_weight, preferred_element_type=jnp.float32)]
    another operation x6 -> x0, local copies, waits for them, and re-layouts: 4.04 us -> none  [the longest x1 1.08 us: body(): key_heads = key_cache.reshape(seq_count, span, head_count, head_size)]
    all_to_all x3 -> x0, other arithmetic: 3.04 us -> none  [the longest x1 1.7 us: copy_for_each(): return lax.all_to_all(copies, axis, split_axis=0, concat_axis=0, tiled=True)]
    slice x24 -> x0, local copies, waits for them, and re-layouts: 2.86 us -> none  [the longest x20 2.07 us: combined_pairwise(): part[side::2]]
    add x12 -> x0, other arithmetic: 1.72 us -> none  [the longest x6 1.63 us: combine_parts(): first[2] * first_scale[:, :, None] + second[2] * second_scale[:, :, None]]
  transfers between devices with their start and end apart: 5 -> 0, of which waited for: 5 -> 0; matrix products, arithmetic and copies ran while one was open for 8% -> 0% of each run, Pallas kernels for 0% -> 0%
where the time goes in v1:
time: 55.2 us; the launch traced here: 54.8 us
  Pallas kernels  48.4 us (88%)
  local copies, waits for them, and re-layouts  5.81 us (11%)
  between operations  0.64 us (1%)
    pallas_call x1, Pallas kernels, body(): pl.pallas_call(kernel, out_shape=(jax.ShapeDtypeStruct((2, 256, 256), BF1...  48.4 us
    unnamed x4, local copies, waits for them, and re-layouts  5.81 us

profile of v1, /device:TPU:1, one launch (start us, length us, event | category | flops | bytes accessed | tf_op | source)
XLA Modules:
  0.0 54.8 jit_solution(16679119080931868742)
XLA Ops:
  0.6 48.4 %shard_map.111 = (bf16[2,256,256]{2,1,0:T(8,128)(2,1)}, bf16[2,256,256]{2,1,0:T(8,128)(2,1)}, f32[2,4,256]{2,1,0:T(4,128)}, bf16[2,32]{1,0:T(2,128)(2,1)}) custom-call(bf16[2,256,2048]{2,1,0:T(8,128)(2,1)} %tok_hbm.1, bf16[2048,256]{1,0:T(8,128)(2,1)} %wk_hbm.1, bf16[2048,256]{1,0:T(8,128)(2,1)} %wv_hbm.1, f32[2,4,256]{2,1,0:T(4,128)} %bitcast.16, ...), custom_call_target="tpu_custom_call" | custom-call | tf_op jit(solution)/shard_map/pallas_call | solution.py:375
  49.0 1.7 %copy.19 = bf16[2,1,256,256]{3,2,1,0:T(8,128)(2,1)} copy(bf16[2,1,256,256]{3,2,1,0:T(8,128)(2,1)} %bitcast.14) | data formatting | bytes 524288
  50.7 1.7 %copy.20 = bf16[2,1,256,256]{3,2,1,0:T(8,128)(2,1)} copy(bf16[2,1,256,256]{3,2,1,0:T(8,128)(2,1)} %bitcast.13) | data formatting | bytes 524288
  52.4 1.3 %copy.21 = f32[2,1,256,4]{2,3,1,0:T(4,128)} copy(f32[2,1,256,4]{2,3,1,0:T(4,128)} %bitcast.17) | data formatting | bytes 16384
  53.6 1.2 %copy.22 = bf16[2,32]{1,0:T(2,128)(2,1)} copy(bf16[2,32]{1,0:T(2,128)(2,1)} %get-tuple-element.23) | data formatting | bytes 256

commit v2 on v1

--- a/solution.py
+++ b/solution.py
@@ -11,8 +11,6 @@
 BF16 = jnp.bfloat16
 NZ, NY, NX, NC = 16, 4, 4, 2
 HIGH = lax.Precision.HIGHEST
-
-ORDER = (1, 2, 3, 4, 8, 7, 6, 5)
 
 
 def slots_of(d):
@@ -52,10 +50,11 @@
 
 
 def kernel(
-    tok_hbm, wk_hbm, wv_hbm, gate_ref, new_in_ref, query_ref, new_gate_ref, ow_ref,
+    tok_hbm, wk_hbm, wv_hbm, gate_hbm, new_in_hbm, query_hbm, new_gate_hbm, ow_hbm,
     k_out, v_out, g_out, m_out,
-    tok, wk, wv, part, sent, zbuf, tbuf, g8, pg, zg, yg, ap, ay, azs, az, afs, af, tps, tpr, kv_loc,
-    sem_in, d_sem, zs_sem, ys_sem, xs_sem, cs_sem, zr_sem, yr_sem, xr_sem, cr_sem,
+    tok, wk, wv, part, gate_ref, new_in_ref, query_ref, new_gate_ref, ow_ref,
+    order, sent, tbuf, g8, pg, zg, yg, ap, ay, azs, az, afs, af, tps, tpr, kv_loc,
+    sem_in, d_sem, zs_sem, ys_sem, xs_sem, cs_sem, zr_sem, xl_sem, xh_sem, x2_sem, cr_sem,
     gzs_sem, gzr_sem, gys_sem, gyr_sem, a_send, a_recv,
 ):
     z, y = lax.axis_index("z"), lax.axis_index("y")
@@ -69,7 +68,7 @@
         return lax.rem(y + d, NY)
 
     def xat(d):
-        return lax.rem(x + d, NX)
+        return lax.rem(x + (d + NX), NX)
 
     def remote(src, dst, ssem, rsem, **dev):
         return pltpu.make_async_remote_copy(
@@ -85,82 +84,72 @@
 
     barrier = pltpu.get_barrier_semaphore()
     cols = pl.ds(pl.multiple_of(me * 256, 256), 256)
-    load_part = pltpu.make_async_copy(tok_hbm.at[:, :, cols], part, sem_in.at[0])
-    load_tok = pltpu.make_async_copy(tok_hbm, tok, sem_in.at[1])
-    load_wk = pltpu.make_async_copy(wk_hbm, wk, sem_in.at[2])
-    load_wv = pltpu.make_async_copy(wv_hbm, wv, sem_in.at[3])
+    sources = (
+        (tok_hbm.at[:, :, cols], part), (tok_hbm, tok), (wk_hbm, wk), (wv_hbm, wv),
+        (gate_hbm, gate_ref), (new_in_hbm, new_in_ref), (query_hbm, query_ref),
+        (new_gate_hbm, new_gate_ref), (ow_hbm, ow_ref),
+    )
+    loads = [pltpu.make_async_copy(s, d, sem_in.at[k]) for k, (s, d) in enumerate(sources)]
+    load_part, load_tok, load_wk, load_wv, load_gate, load_in, load_q, load_ng, load_ow = loads
     load_part.start()
+    for dz in (1, -1):
+        for dy in range(NY):
+            signal(barrier, z=zat(dz), y=yat(dy))
     for dy in range(1, NY):
         signal(barrier, y=yat(dy))
     for dx in range(NX):
         for dc in range(NC):
             if dx or dc:
                 signal(barrier, x=xat(dx), c=lax.rem(c + dc, NC))
-    for dz in (1, -1):
-        signal(barrier, z=zat(dz))
-    load_wk.start()
-    load_tok.start()
-    load_wv.start()
-
-    o, i = iota((512, 512), 0), iota((512, 512), 1)
-    perm = (i == ((o & 4) << 6) + ((o & 3) << 6) + (o >> 3)).astype(F32).astype(BF16)
-    load_part.wait()
-    moved = jnp.dot(perm, part[...].reshape(512, 256), preferred_element_type=F32)
-    sent[...] = moved.reshape(NZ, NY, 8, 256).astype(BF16)
-
-    g8[0:4, :] = gate_ref[0]
-    g8[4:8, :] = gate_ref[1]
-    gates = g8[...]
-    lanes, rows = iota((128, 256), 1), iota((128, 256), 0)
-    spread = jnp.concatenate(
-        [jnp.broadcast_to(gates[k : k + 1, :], (16, 256)) for k in range(8)], axis=0
-    )
-    same = ((lanes & 3) == ((rows >> 2) & 3)) & ((lanes >> 6) == (rows & 3))
-    spread = jnp.where(same, spread, 0.0)
-    pick = ((iota((16, 256), 1) >> 2) & 15) == iota((16, 256), 0)
-    gate_rows = nt_dot(pick.astype(F32), spread, HIGH)
-    for k in range(NZ):
-        pg[k] = gate_rows[k : k + 1, :]
+    for load in (load_gate, load_q, load_ng, load_in, load_wk, load_tok, load_wv, load_ow):
+        load.start()
 
     def send_z(d):
         for sign in (1, -1) if d < NZ // 2 else (1,):
             first, count = slots_of(d)
             slot = first if sign < 0 or count == 1 else first + 1
-            remote(
-                sent.at[zat(sign * d)], zbuf.at[slot], zs_sem, zr_sem.at[d], z=zat(sign * d)
-            ).start()
-            remote(pg.at[zat(sign * d)], zg.at[z], gzs_sem, gzr_sem, z=zat(sign * d)).start()
+            to = zat(sign * d)
+            for dy in range(NY):
+                remote(
+                    sent.at[to, yat(dy)], tbuf.at[me, slot, y], zs_sem, zr_sem.at[d],
+                    z=to, y=yat(dy),
+                ).start()
 
     def slots(d):
         first, count = slots_of(d)
         return pl.ds(first, count)
 
-    def y_forward(d):
+    def half(f, d, upper):
+        first, count = slots_of(d)
+        if count == 2:
+            return tbuf.at[f, pl.ds(first + upper, 1)]
+        return tbuf.at[f, pl.ds(first, 1), pl.ds(2 * upper, 2)]
+
+    low_f, high_f = xat(-1) * NC + c, xat(1) * NC + c
+
+    def x_first(d):
+        here = tbuf.at[me, slots(d)]
         if d:
-            wait_bytes(zbuf.at[slots(d)], zr_sem.at[d])
-        for dy in range(1, NY):
-            remote(
-                zbuf.at[slots(d), yat(dy)], tbuf.at[me, slots(d), y], ys_sem, yr_sem.at[d],
-                y=yat(dy),
-            ).start()
-        tbuf[me, slots(d), y] = zbuf[slots(d), y]
-
-    def x_forward(d):
-        wait_bytes(zbuf.at[slots(d), pl.ds(0, 3)], yr_sem.at[d])
-        here = tbuf.at[me, slots(d)]
-        for dx in range(1, NX):
-            remote(here, here, xs_sem, xr_sem.at[d], x=xat(dx)).start()
+            wait_bytes(here, zr_sem.at[d])
+        else:
+            wait_bytes(tbuf.at[me, 0, pl.ds(0, 3)], zr_sem.at[0])
+        remote(here, here, xs_sem, xl_sem.at[d], x=xat(1)).start()
+        remote(here, here, xs_sem, xh_sem.at[d], x=xat(-1)).start()
         remote(here, here, cs_sem, cr_sem.at[d], c=1 - c).start()
 
-    def c_forward(d):
-        wait_bytes(tbuf.at[pl.ds(0, 3), slots(d)], xr_sem.at[d])
-        for dx in range(1, NX):
-            there = tbuf.at[xat(dx) * NC + c, slots(d)]
-            remote(there, there, cs_sem, cr_sem.at[d], c=1 - c).start()
+    def x_second(d):
+        for f, sem, upper, to in ((low_f, xl_sem, 0, xat(1)), (high_f, xh_sem, 1, xat(-1))):
+            came = tbuf.at[f, slots(d)]
+            wait_bytes(came, sem.at[d])
+            piece = half(f, d, upper)
+            for core in range(NC):
+                remote(piece, piece, xs_sem, x2_sem.at[d], x=to, c=lax.rem(c + core, NC)).start()
+            remote(came, came, cs_sem, cr_sem.at[d], c=1 - c).start()
 
     def finish(ds):
         for d in ds:
-            wait_bytes(tbuf.at[pl.ds(0, 4), slots(d)], cr_sem.at[d])
+            wait_bytes(tbuf.at[pl.ds(0, 3), slots(d)], cr_sem.at[d])
+            wait_bytes(tbuf.at[pl.ds(0, 2), slots(d)], x2_sem.at[d])
         first = min(slots_of(d)[0] for d in ds)
         count = sum(slots_of(d)[1] for d in ds)
         for w, out in ((wk, k_out), (wv, v_out)):
@@ -187,18 +176,44 @@
                     at = pl.multiple_of(zat(rel) * 16, 16)
                     out[b, pl.ds(at, 16), :] = block[k]
 
-    pl.semaphore_wait(barrier, 3 + 7 + 2)
+    pl.semaphore_wait(barrier, 3 + 7 + 8)
     for s in (1, -1):
         signal(d_sem.at[0], z=zat(s))
+    load_part.wait()
+    for b in range(2):
+        for j in range(4):
+            for k in range(2):
+                order[k, pl.ds(4 * b + j, 64, stride=8), :] = part[
+                    b, 64 * j : 64 * j + 64, 128 * k : 128 * k + 128
+                ].astype(F32)
+    for k in range(2):
+        sent[:, :, :, 128 * k : 128 * k + 128] = order[k].reshape(NZ, NY, 8, 128).astype(BF16)
+    for dy in range(1, NY):
+        remote(
+            sent.at[z, yat(dy)], tbuf.at[me, 0, y], ys_sem, zr_sem.at[0], y=yat(dy)
+        ).start()
     send_z(1)
-    zbuf[0] = sent[z]
-    zg[z] = pg[z]
-    y_forward(0)
+    tbuf[me, 0, y] = sent[z, y]
     pl.semaphore_wait(d_sem.at[0], 2)
     for s in (2, -2):
         signal(d_sem.at[1], z=zat(s))
     send_z(2)
 
+    load_gate.wait()
+    g8[0:4, :] = gate_ref[0]
+    g8[4:8, :] = gate_ref[1]
+    gates = g8[...]
+    lanes, rows = iota((128, 256), 1), iota((128, 256), 0)
+    spread = jnp.concatenate(
+        [jnp.broadcast_to(gates[k : k + 1, :], (16, 256)) for k in range(8)], axis=0
+    )
+    same = ((lanes & 3) == ((rows >> 2) & 3)) & ((lanes >> 6) == (rows & 3))
+    spread = jnp.where(same, spread, 0.0)
+    pick = ((iota((16, 256), 1) >> 2) & 15) == iota((16, 256), 0)
+    gate_rows = nt_dot(pick.astype(F32), spread, HIGH)
+    for k in range(NZ):
+        pg[k] = gate_rows[k : k + 1, :]
+
     head_of_row = iota((8, 256), 0) & 3
     mine = (iota((8, 256), 1) >> 6) == head_of_row
     second = iota((8, 256), 0) >= 4
@@ -208,20 +223,24 @@
             second, jnp.broadcast_to(two[1:2, :], (8, 256)), jnp.broadcast_to(two[0:1, :], (8, 256))
         )
 
+    for load in (load_q, load_ng, load_in):
+        load.wait()
     query = jnp.where(mine, by_row(query_ref[...].astype(F32)), 0.0)
     query_b = query.astype(BF16)
-    load_wk.wait()
-    load_tok.wait()
     new_in = new_in_ref[...]
-    key_now = jnp.dot(new_in, wk[...], preferred_element_type=F32).astype(BF16).astype(F32)
-    local = tok[...].reshape(512, 2048)
-    kv_loc[...] = jnp.dot(local, wk[...], preferred_element_type=F32).astype(BF16)
     pl.semaphore_wait(d_sem.at[1], 2)
     for s in (4, -4):
         signal(d_sem.at[2], z=zat(s))
     send_z(3)
     send_z(4)
-    y_forward(1)
+    x_first(0)
+    x_first(1)
+    load_wk.wait()
+    load_tok.wait()
+    key_now = jnp.dot(new_in, wk[...], preferred_element_type=F32).astype(BF16).astype(F32)
+    local = tok[...].reshape(512, 2048)
+    kv_loc[...] = jnp.dot(local, wk[...], preferred_element_type=F32).astype(BF16)
+    x_second(0)
     raw = jnp.where(
         second, nt_dot(query_b, kv_loc[256:, :]), nt_dot(query_b, kv_loc[:256, :])
     )
@@ -240,9 +259,9 @@
     total = jnp.sum(expo, axis=1, keepdims=True)
     expo_b = expo.astype(BF16)
     load_wv.wait()
-    value_now = jnp.dot(new_in, wv[...], preferred_element_type=F32).astype(BF16).astype(F32)
     kv_loc[...] = jnp.dot(local, wv[...], preferred_element_type=F32).astype(BF16)
-    x_forward(0)
+    x_first(2)
+    x_second(1)
     num = jnp.where(
         second,
         jnp.dot(expo_b, kv_loc[256:, :], preferred_element_type=F32),
@@ -258,11 +277,15 @@
     for dy in range(1, NY):
         remote(ap.at[yat(dy)], ay.at[y], a_send.at[0], a_recv.at[0], y=yat(dy)).start()
     ay[y] = ap[y]
-    y_forward(2)
     pl.semaphore_wait(d_sem.at[2], 2)
     send_z(8)
     send_z(7)
-    x_forward(1)
+    zg[z] = pg[z]
+    for d in range(1, NZ):
+        remote(pg.at[zat(d)], zg.at[z], gzs_sem, gzr_sem, z=zat(d)).start()
+    value_now = jnp.dot(new_in, wv[...], preferred_element_type=F32).astype(BF16).astype(F32)
+    x_first(3)
+    x_second(2)
     wait_bytes(ay.at[pl.ds(0, 3)], a_recv.at[0])
     merged = merge([ay[k] for k in range(NY)])
     azs[...] = merged
@@ -271,37 +294,28 @@
         remote(azs, az.at[z], a_send.at[1], a_recv.at[1], z=zat(d)).start()
     send_z(6)
     send_z(5)
-
-    y_forward(3)
-    c_forward(0)
-    x_forward(2)
-    y_forward(4)
-    c_forward(1)
-    x_forward(3)
-    c_forward(2)
-    x_forward(4)
-    c_forward(3)
-    c_forward(4)
-    finish((0, 1, 2, 3, 4))
-    y_forward(8)
-    y_forward(7)
-    x_forward(8)
+    x_first(4)
+    x_second(3)
+    finish((0, 1, 2, 3))
+    x_second(4)
+    x_first(8)
+    x_first(7)
     wait_bytes(az.at[pl.ds(0, 15)], a_recv.at[1])
     merged = merge([az[k] for k in range(NZ)])
     afs[...] = merged
     af[y] = merged
     for dy in range(1, NY):
         remote(afs, af.at[y], a_send.at[2], a_recv.at[2], y=yat(dy)).start()
-    y_forward(6)
-    x_forward(7)
-    y_forward(5)
+    x_second(8)
+    x_first(6)
     wait_bytes(zg.at[pl.ds(0, 15)], gzr_sem)
     for dy in range(1, NY):
         remote(zg, yg.at[y], gys_sem, gyr_sem, y=yat(dy)).start()
     for k in range(NZ):
         yg[y, k] = zg[k]
-    c_forward(8)
-    x_forward(6)
+    x_second(7)
+    x_first(5)
+    load_ow.wait()
     wait_bytes(af.at[pl.ds(0, 3)], a_recv.at[2])
     cached = jnp.concatenate([af[k] for k in range(NY)], axis=0)
     own = jnp.sum(query * by_row(key_now), axis=1, keepdims=True) * 0.125
@@ -330,9 +344,8 @@
                     tps, tpr.at[me], a_send.at[3], a_recv.at[3],
                     x=xat(dx), c=lax.rem(c + dc, NC),
                 ).start()
-    x_forward(5)
-    c_forward(7)
-    c_forward(6)
+    x_second(6)
+    x_second(5)
     wait_bytes(yg.at[pl.ds(0, 3)], gyr_sem)
     field = (iota((16, 128), 1) >> 2) & 3
     gathered = jnp.zeros((16, 128), F32)
@@ -354,12 +367,11 @@
     for k in range(1, NX * NC):
         mixed += tpr[k]
     m_out[...] = mixed[:, :32].astype(BF16)
-    c_forward(5)
-    finish((5, 6, 7, 8))
-    wait_bytes(zbuf.at[pl.ds(0, 15)], zs_sem)
-    wait_bytes(zbuf.at[pl.ds(0, 12)], ys_sem)
-    wait_bytes(tbuf.at[pl.ds(0, 3)], xs_sem)
-    wait_bytes(tbuf.at[pl.ds(0, 4)], cs_sem)
+    finish((4, 5, 6, 7, 8))
+    wait_bytes(tbuf.at[0, pl.ds(0, 15)], zs_sem)
+    wait_bytes(tbuf.at[0, 0, pl.ds(0, 3)], ys_sem)
+    wait_bytes(tbuf.at[pl.ds(0, 4)], xs_sem)
+    wait_bytes(tbuf.at[pl.ds(0, 3)], cs_sem)
     wait_bytes(zg.at[pl.ds(0, 15)], gzs_sem)
     wait_bytes(yg.at[pl.ds(0, 3)], gys_sem)
     wait_bytes(ap.at[pl.ds(0, 3)], a_send.at[0])
@@ -368,26 +380,43 @@
     wait_bytes(tpr.at[pl.ds(0, 7)], a_send.at[3])
 
 
+def put_out(*refs):
+    ins, outs, sem = refs[:4], refs[4:8], refs[8]
+    copies = [
+        pltpu.make_async_copy(i, o, sem.at[k]) for k, (i, o) in enumerate(zip(ins, outs))
+    ]
+    for copy in copies:
+        copy.start()
+    for copy in copies:
+        copy.wait()
+
+
 def body(tokens, key_weight, value_weight, cum_gate, new_input, new_query, new_gate, out_weight):
     vmem = pl.BlockSpec(memory_space=pltpu.VMEM)
-    hbm = pl.BlockSpec(memory_space=pl.ANY)
+    hbm = pl.BlockSpec(memory_space=pltpu.HBM)
     dma, regular = pltpu.SemaphoreType.DMA, pltpu.SemaphoreType.REGULAR
-    keys, values, gates, mixed = pl.pallas_call(
+    shapes = (
+        jax.ShapeDtypeStruct((2, 256, 256), BF16),
+        jax.ShapeDtypeStruct((2, 256, 256), BF16),
+        jax.ShapeDtypeStruct((2, 4, 256), F32),
+        jax.ShapeDtypeStruct((2, 32), BF16),
+    )
+    results = pl.pallas_call(
         kernel,
-        out_shape=(
-            jax.ShapeDtypeStruct((2, 256, 256), BF16),
-            jax.ShapeDtypeStruct((2, 256, 256), BF16),
-            jax.ShapeDtypeStruct((2, 4, 256), F32),
-            jax.ShapeDtypeStruct((2, 32), BF16),
-        ),
-        in_specs=[hbm, hbm, hbm, vmem, vmem, vmem, vmem, vmem],
-        out_specs=(vmem, vmem, vmem, vmem),
+        out_shape=shapes,
+        in_specs=[hbm] * 8,
+        out_specs=(vmem,) * 4,
         scratch_shapes=[
             pltpu.VMEM((2, 256, 2048), BF16),
             pltpu.VMEM((2048, 256), BF16),
             pltpu.VMEM((2048, 256), BF16),
             pltpu.VMEM((2, 256, 256), BF16),
-            pltpu.VMEM((NZ, NY, 8, 256), BF16),
+            pltpu.VMEM((2, 4, 256), F32),
+            pltpu.VMEM((2, 2048), BF16),
+            pltpu.VMEM((2, 256), BF16),
+            pltpu.VMEM((2, 4), F32),
+            pltpu.VMEM((32, 256), BF16),
+            pltpu.VMEM((2, 512, 128), F32),
             pltpu.VMEM((NZ, NY, 8, 256), BF16),
             pltpu.VMEM((8, NZ, NY, 8, 256), BF16),
             pltpu.VMEM((8, 256), F32),
@@ -403,18 +432,33 @@
             pltpu.VMEM((2, 128), F32),
             pltpu.VMEM((8, 2, 128), F32),
             pltpu.VMEM((512, 256), BF16),
-            dma((4,)),
+            dma((9,)),
             regular((3,)),
             dma, dma, dma, dma,
-            dma((9,)), dma((9,)), dma((9,)), dma((9,)),
+            dma((9,)), dma((9,)), dma((9,)), dma((9,)), dma((9,)),
             dma, dma, dma, dma,
             dma((4,)), dma((4,)),
         ],
-        compiler_params=pltpu.CompilerParams(collective_id=0, has_side_effects=True),
+        compiler_params=pltpu.CompilerParams(
+            collective_id=0, has_side_effects=True, vmem_limit_bytes=24 * 2**20
+        ),
     )(
-        tokens, key_weight, value_weight, jnp.swapaxes(cum_gate, 1, 2), new_input, new_query,
-        new_gate, out_weight.T,
-    )
+        *(
+            pltpu.with_memory_space_constraint(a, pltpu.HBM)
+            for a in (
+                tokens, key_weight, value_weight, jnp.swapaxes(cum_gate, 1, 2), new_input,
+                new_query, new_gate, out_weight.T,
+            )
+        )
+    )
+    keys, values, gates, mixed = pl.pallas_call(
+        put_out,
+        out_shape=shapes,
+        in_specs=[vmem] * 4,
+        out_specs=(hbm,) * 4,
+        scratch_shapes=[dma((4,))],
+        compiler_params=pltpu.CompilerParams(vmem_limit_bytes=4 * 2**20),
+    )(*results)
     return (
         keys.reshape(2, 1, 256, 256),
         values.reshape(2, 1, 256, 256),

time: 55.2 us -> 47.2 us (0.86)
  local copies, waits for them, and re-layouts: 5.81 us -> 0 us
  Pallas kernels: 48.4 us -> 46.4 us
    unnamed x4 -> x0, local copies, waits for them, and re-layouts: 5.81 us -> none
    pallas_call x1 -> x2, Pallas kernels: 48.4 us -> 46.4 us  [the longest x1 45.6 us: body(): pl.pallas_call(kernel, out_shape=shapes, in_specs=[hbm] * 8, out_specs=(v...]
where the time goes in v2:
time: 47.2 us; the launch traced here: 47.1 us
  Pallas kernels  46.4 us (98%)
  between operations  0.64 us (1%)
    pallas_call x1, Pallas kernels, body(): pl.pallas_call(kernel, out_shape=shapes, in_specs=[hbm] * 8, out_specs=(v...  45.6 us

profile of v2, /device:TPU:1, one launch (start us, length us, event | category | flops | bytes accessed | tf_op | source)
XLA Modules:
  0.0 47.1 jit_solution(16061751817469645909)
XLA Ops:
  0.6 45.6 %shard_map.111 = (bf16[2,256,256]{2,1,0:T(8,128)(2,1)S(1)}, bf16[2,256,256]{2,1,0:T(8,128)(2,1)S(1)}, f32[2,4,256]{2,1,0:T(4,128)S(1)}, bf16[2,32]{1,0:T(2,128)(2,1)S(1)}) custom-call(bf16[2,256,2048]{2,1,0:T(8,128)(2,1)} %tok_hbm.1, bf16[2048,256]{1,0:T(8,128)(2,1)} %wk_hbm.1, bf16[2048,256]{1,0:T(8,128)(2,1)} %wv_hbm.1, f32[2,4,256]{2,1,0:T(4,128)} %bitcast.14, ...), custom_call_target="tpu_custom_call" | custom-call | tf_op jit(solution)/shard_map/pallas_call | solution.py:404
  46.2 0.8 %shard_map.112 = (bf16[2,256,256]{2,1,0:T(8,128)(2,1)}, bf16[2,256,256]{2,1,0:T(8,128)(2,1)}, f32[2,4,256]{2,1,0:T(4,128)}, bf16[2,32]{1,0:T(2,128)(2,1)}) custom-call(bf16[2,256,256]{2,1,0:T(8,128)(2,1)S(1)} %get-tuple-element.12.refs_0_, bf16[2,256,256]{2,1,0:T(8,128)(2,1)S(1)} %get-tuple-element.13.refs_1_, f32[2,4,256]{2,1,0:T(4,128)S(1)} %get-tuple-element.14.refs_2_, ...), custom_call_target="tpu_custom_call" | custom-call | tf_op jit(solution)/shard_map/pallas_call | solution.py:454

commit v3 on v2

--- a/solution.py
+++ b/solution.py
@@ -11,6 +11,7 @@
 BF16 = jnp.bfloat16
 NZ, NY, NX, NC = 16, 4, 4, 2
 HIGH = lax.Precision.HIGHEST
+FAR = 4
 
 
 def slots_of(d):
@@ -53,9 +54,9 @@
     tok_hbm, wk_hbm, wv_hbm, gate_hbm, new_in_hbm, query_hbm, new_gate_hbm, ow_hbm,
     k_out, v_out, g_out, m_out,
     tok, wk, wv, part, gate_ref, new_in_ref, query_ref, new_gate_ref, ow_ref,
-    order, sent, tbuf, g8, pg, zg, yg, ap, ay, azs, az, afs, af, tps, tpr, kv_loc,
-    sem_in, d_sem, zs_sem, ys_sem, xs_sem, cs_sem, zr_sem, xl_sem, xh_sem, x2_sem, cr_sem,
-    gzs_sem, gzr_sem, gys_sem, gyr_sem, a_send, a_recv,
+    order, sent, tbuf, relay, g8, pg, zg, yg, grelay, azs, az, far, afs, af, tps, tpr, kv_loc,
+    sem_in, d_sem, zs_sem, ys_sem, ls_sem, rs_sem, xs_sem, cs_sem, zr_sem, lr_sem, xr_sem, cr_sem,
+    gzs_sem, gzr_sem, grs_sem, grr_sem, gys_sem, gyr_sem, a_send, a_recv,
 ):
     z, y = lax.axis_index("z"), lax.axis_index("y")
     x, c = lax.axis_index("x"), lax.axis_index("c")
@@ -104,28 +105,41 @@
     for load in (load_gate, load_q, load_ng, load_in, load_wk, load_tok, load_wv, load_ow):
         load.start()
 
+    def slot_at(d, sign):
+        first, count = slots_of(d)
+        return first + 1 if sign > 0 and count == 2 else first
+
     def send_z(d):
-        for sign in (1, -1) if d < NZ // 2 else (1,):
-            first, count = slots_of(d)
-            slot = first if sign < 0 or count == 1 else first + 1
+        for sign in (1, -1):
             to = zat(sign * d)
             for dy in range(NY):
                 remote(
-                    sent.at[to, yat(dy)], tbuf.at[me, slot, y], zs_sem, zr_sem.at[d],
+                    sent.at[to, yat(dy)], tbuf.at[me, slot_at(d, sign), y], zs_sem, zr_sem.at[d],
                     z=to, y=yat(dy),
+                ).start()
+
+    def to_relay(k):
+        for way, sign in enumerate((1, -1)):
+            to = zat(sign * (FAR + k))
+            if k < FAR:
+                src, dst = sent.at[to], relay.at[way, k - 1]
+            else:
+                src, dst = sent.at[to, pl.ds(2 * way, 2)], relay.at[way, k - 1, pl.ds(0, 2)]
+            remote(src, dst, ls_sem, lr_sem.at[k], z=zat(sign * FAR)).start()
+
+    def pass_on(k):
+        came = relay.at[:, k - 1] if k < FAR else relay.at[:, k - 1, pl.ds(0, 2)]
+        wait_bytes(came, lr_sem.at[k])
+        for way, sign in enumerate((1, -1)):
+            for q in range(NY if k < FAR else 2):
+                remote(
+                    relay.at[way, k - 1, q], tbuf.at[me, slot_at(FAR + k, sign), y], rs_sem,
+                    zr_sem.at[FAR + k], z=zat(sign * k), y=q if k < FAR else q + 2 * way,
                 ).start()
 
     def slots(d):
         first, count = slots_of(d)
         return pl.ds(first, count)
-
-    def half(f, d, upper):
-        first, count = slots_of(d)
-        if count == 2:
-            return tbuf.at[f, pl.ds(first + upper, 1)]
-        return tbuf.at[f, pl.ds(first, 1), pl.ds(2 * upper, 2)]
-
-    low_f, high_f = xat(-1) * NC + c, xat(1) * NC + c
 
     def x_first(d):
         here = tbuf.at[me, slots(d)]
@@ -133,23 +147,19 @@
             wait_bytes(here, zr_sem.at[d])
         else:
             wait_bytes(tbuf.at[me, 0, pl.ds(0, 3)], zr_sem.at[0])
-        remote(here, here, xs_sem, xl_sem.at[d], x=xat(1)).start()
-        remote(here, here, xs_sem, xh_sem.at[d], x=xat(-1)).start()
+        for dx in (1, -1, 2):
+            remote(here, here, xs_sem, xr_sem.at[d], x=xat(dx)).start()
         remote(here, here, cs_sem, cr_sem.at[d], c=1 - c).start()
 
     def x_second(d):
-        for f, sem, upper, to in ((low_f, xl_sem, 0, xat(1)), (high_f, xh_sem, 1, xat(-1))):
-            came = tbuf.at[f, slots(d)]
-            wait_bytes(came, sem.at[d])
-            piece = half(f, d, upper)
-            for core in range(NC):
-                remote(piece, piece, xs_sem, x2_sem.at[d], x=to, c=lax.rem(c + core, NC)).start()
+        wait_bytes(tbuf.at[pl.ds(0, 3), slots(d)], xr_sem.at[d])
+        for dx in range(1, NX):
+            came = tbuf.at[xat(dx) * NC + c, slots(d)]
             remote(came, came, cs_sem, cr_sem.at[d], c=1 - c).start()
 
     def finish(ds):
         for d in ds:
-            wait_bytes(tbuf.at[pl.ds(0, 3), slots(d)], cr_sem.at[d])
-            wait_bytes(tbuf.at[pl.ds(0, 2), slots(d)], x2_sem.at[d])
+            wait_bytes(tbuf.at[pl.ds(0, 4), slots(d)], cr_sem.at[d])
         first = min(slots_of(d)[0] for d in ds)
         count = sum(slots_of(d)[1] for d in ds)
         for w, out in ((wk, k_out), (wv, v_out)):
@@ -199,6 +209,23 @@
         signal(d_sem.at[1], z=zat(s))
     send_z(2)
 
+    pl.semaphore_wait(d_sem.at[1], 2)
+    to_relay(1)
+    to_relay(2)
+    head_of_row = iota((8, 256), 0) & 3
+    mine = (iota((8, 256), 1) >> 6) == head_of_row
+    second = iota((8, 256), 0) >= 4
+
+    def by_row(two):
+        return jnp.where(
+            second, jnp.broadcast_to(two[1:2, :], (8, 256)), jnp.broadcast_to(two[0:1, :], (8, 256))
+        )
+
+    for load in (load_q, load_ng, load_in):
+        load.wait()
+    query = jnp.where(mine, by_row(query_ref[...].astype(F32)), 0.0)
+    query_b = query.astype(BF16)
+    new_in = new_in_ref[...]
     load_gate.wait()
     g8[0:4, :] = gate_ref[0]
     g8[4:8, :] = gate_ref[1]
@@ -214,33 +241,12 @@
     for k in range(NZ):
         pg[k] = gate_rows[k : k + 1, :]
 
-    head_of_row = iota((8, 256), 0) & 3
-    mine = (iota((8, 256), 1) >> 6) == head_of_row
-    second = iota((8, 256), 0) >= 4
-
-    def by_row(two):
-        return jnp.where(
-            second, jnp.broadcast_to(two[1:2, :], (8, 256)), jnp.broadcast_to(two[0:1, :], (8, 256))
-        )
-
-    for load in (load_q, load_ng, load_in):
-        load.wait()
-    query = jnp.where(mine, by_row(query_ref[...].astype(F32)), 0.0)
-    query_b = query.astype(BF16)
-    new_in = new_in_ref[...]
-    pl.semaphore_wait(d_sem.at[1], 2)
-    for s in (4, -4):
-        signal(d_sem.at[2], z=zat(s))
-    send_z(3)
-    send_z(4)
-    x_first(0)
-    x_first(1)
+    to_relay(4)
     load_wk.wait()
     load_tok.wait()
     key_now = jnp.dot(new_in, wk[...], preferred_element_type=F32).astype(BF16).astype(F32)
     local = tok[...].reshape(512, 2048)
     kv_loc[...] = jnp.dot(local, wk[...], preferred_element_type=F32).astype(BF16)
-    x_second(0)
     raw = jnp.where(
         second, nt_dot(query_b, kv_loc[256:, :]), nt_dot(query_b, kv_loc[:256, :])
     )
@@ -258,10 +264,12 @@
     expo = jnp.exp(scores - top)
     total = jnp.sum(expo, axis=1, keepdims=True)
     expo_b = expo.astype(BF16)
+    x_first(1)
+    x_first(0)
     load_wv.wait()
     kv_loc[...] = jnp.dot(local, wv[...], preferred_element_type=F32).astype(BF16)
     x_first(2)
-    x_second(1)
+    send_z(3)
     num = jnp.where(
         second,
         jnp.dot(expo_b, kv_loc[256:, :], preferred_element_type=F32),
@@ -272,52 +280,61 @@
     packed = jnp.where(
         lane < 64, num, jnp.where(lane == 64, total, jnp.where(lane == 65, top, 0.0))
     )
-    for k in range(NY):
-        ap[k] = packed[2 * k : 2 * k + 2, :]
-    for dy in range(1, NY):
-        remote(ap.at[yat(dy)], ay.at[y], a_send.at[0], a_recv.at[0], y=yat(dy)).start()
-    ay[y] = ap[y]
-    pl.semaphore_wait(d_sem.at[2], 2)
-    send_z(8)
-    send_z(7)
+    azs[...] = packed
+    for d in range(1, FAR + 1):
+        for sign in (1, -1):
+            slot = d - 1 if sign < 0 else FAR + d - 1
+            remote(azs, az.at[slot], a_send.at[0], a_recv.at[0], z=zat(sign * d)).start()
+    to_relay(3)
+    x_second(0)
+    x_second(1)
+    pass_on(1)
+    send_z(4)
+    pass_on(2)
+    x_first(3)
     zg[z] = pg[z]
-    for d in range(1, NZ):
-        remote(pg.at[zat(d)], zg.at[z], gzs_sem, gzr_sem, z=zat(d)).start()
-    value_now = jnp.dot(new_in, wv[...], preferred_element_type=F32).astype(BF16).astype(F32)
-    x_first(3)
-    x_second(2)
-    wait_bytes(ay.at[pl.ds(0, 3)], a_recv.at[0])
-    merged = merge([ay[k] for k in range(NY)])
-    azs[...] = merged
-    az[z] = merged
-    for d in range(1, NZ):
-        remote(azs, az.at[z], a_send.at[1], a_recv.at[1], z=zat(d)).start()
-    send_z(6)
-    send_z(5)
+    for sign in (1, -1):
+        for d in range(1, FAR + 1):
+            remote(pg.at[zat(sign * d)], zg.at[z], gzs_sem, gzr_sem, z=zat(sign * d)).start()
+    for way, sign in enumerate((1, -1)):
+        for k in range(1, FAR + 1 - way):
+            remote(
+                pg.at[zat(sign * (FAR + k))], grelay.at[FAR * way + k - 1], gzs_sem, grr_sem,
+                z=zat(sign * FAR),
+            ).start()
+    wait_bytes(az.at[pl.ds(0, 8)], a_recv.at[0])
+    far[0] = merge([az[k] for k in range(FAR)])
+    far[1] = merge([az[k] for k in range(FAR, 2 * FAR - 1)])
+    remote(far.at[0], az.at[8], a_send.at[1], a_recv.at[1], z=zat(-FAR)).start()
+    remote(far.at[1], az.at[9], a_send.at[1], a_recv.at[1], z=zat(FAR)).start()
+    pass_on(3)
+    x_first(5)
+    pass_on(4)
+    x_first(6)
     x_first(4)
-    x_second(3)
-    finish((0, 1, 2, 3))
-    x_second(4)
-    x_first(8)
-    x_first(7)
-    wait_bytes(az.at[pl.ds(0, 15)], a_recv.at[1])
-    merged = merge([az[k] for k in range(NZ)])
+    wait_bytes(zg.at[pl.ds(0, 7)], grr_sem)
+    for way, sign in enumerate((1, -1)):
+        for k in range(1, FAR + 1 - way):
+            remote(
+                grelay.at[FAR * way + k - 1], zg.at[zat(-sign * FAR)], grs_sem, gzr_sem,
+                z=zat(sign * k),
+            ).start()
+    wait_bytes(az.at[pl.ds(8, 2)], a_recv.at[1])
+    merged = merge([azs[...]] + [az[k] for k in range(10)])
     afs[...] = merged
     af[y] = merged
     for dy in range(1, NY):
         remote(afs, af.at[y], a_send.at[2], a_recv.at[2], y=yat(dy)).start()
-    x_second(8)
-    x_first(6)
-    wait_bytes(zg.at[pl.ds(0, 15)], gzr_sem)
-    for dy in range(1, NY):
-        remote(zg, yg.at[y], gys_sem, gyr_sem, y=yat(dy)).start()
-    for k in range(NZ):
-        yg[y, k] = zg[k]
-    x_second(7)
-    x_first(5)
+    x_first(7)
+    x_first(8)
+    x_second(2)
+    x_second(3)
+    value_now = jnp.dot(new_in, wv[...], preferred_element_type=F32).astype(BF16).astype(F32)
+    x_second(5)
+    x_second(6)
     load_ow.wait()
     wait_bytes(af.at[pl.ds(0, 3)], a_recv.at[2])
-    cached = jnp.concatenate([af[k] for k in range(NY)], axis=0)
+    cached = merge([af[k] for k in range(NY)])
     own = jnp.sum(query * by_row(key_now), axis=1, keepdims=True) * 0.125
     cached_top, cached_total = cached[:, 65:66], cached[:, 64:65]
     cached_num = jnp.where(lane < 64, cached, pltpu.roll(cached, 64, 1))
@@ -344,8 +361,21 @@
                     tps, tpr.at[me], a_send.at[3], a_recv.at[3],
                     x=xat(dx), c=lax.rem(c + dc, NC),
                 ).start()
-    x_second(6)
-    x_second(5)
+    x_second(4)
+    wait_bytes(zg.at[pl.ds(0, 15)], gzr_sem)
+    for dy in range(1, NY):
+        remote(zg, yg.at[y], gys_sem, gyr_sem, y=yat(dy)).start()
+    for k in range(NZ):
+        yg[y, k] = zg[k]
+    finish((5, 6))
+    finish((0, 1, 2, 3, 4))
+    x_second(7)
+    x_second(8)
+    wait_bytes(tpr.at[pl.ds(0, 7)], a_recv.at[3])
+    mixed = tpr[0]
+    for k in range(1, NX * NC):
+        mixed += tpr[k]
+    m_out[...] = mixed[:, :32].astype(BF16)
     wait_bytes(yg.at[pl.ds(0, 3)], gyr_sem)
     field = (iota((16, 128), 1) >> 2) & 3
     gathered = jnp.zeros((16, 128), F32)
@@ -362,20 +392,18 @@
     gate_cols = nt_dot(pick.astype(F32), spread, HIGH)
     g_out[0] = gate_cols[0:4]
     g_out[1] = gate_cols[4:8]
-    wait_bytes(tpr.at[pl.ds(0, 7)], a_recv.at[3])
-    mixed = tpr[0]
-    for k in range(1, NX * NC):
-        mixed += tpr[k]
-    m_out[...] = mixed[:, :32].astype(BF16)
-    finish((4, 5, 6, 7, 8))
-    wait_bytes(tbuf.at[0, pl.ds(0, 15)], zs_sem)
+    finish((7, 8))
+    wait_bytes(sent.at[pl.ds(0, 8)], zs_sem)
     wait_bytes(tbuf.at[0, 0, pl.ds(0, 3)], ys_sem)
-    wait_bytes(tbuf.at[pl.ds(0, 4)], xs_sem)
-    wait_bytes(tbuf.at[pl.ds(0, 3)], cs_sem)
+    wait_bytes(sent.at[pl.ds(0, 7)], ls_sem)
+    wait_bytes(sent.at[pl.ds(0, 7)], rs_sem)
+    wait_bytes(tbuf.at[pl.ds(0, 3)], xs_sem)
+    wait_bytes(tbuf.at[pl.ds(0, 4)], cs_sem)
     wait_bytes(zg.at[pl.ds(0, 15)], gzs_sem)
+    wait_bytes(zg.at[pl.ds(0, 7)], grs_sem)
     wait_bytes(yg.at[pl.ds(0, 3)], gys_sem)
-    wait_bytes(ap.at[pl.ds(0, 3)], a_send.at[0])
-    wait_bytes(az.at[pl.ds(0, 15)], a_send.at[1])
+    wait_bytes(az.at[pl.ds(0, 8)], a_send.at[0])
+    wait_bytes(far, a_send.at[1])
     wait_bytes(af.at[pl.ds(0, 3)], a_send.at[2])
     wait_bytes(tpr.at[pl.ds(0, 7)], a_send.at[3])
 
@@ -419,24 +447,25 @@
             pltpu.VMEM((2, 512, 128), F32),
             pltpu.VMEM((NZ, NY, 8, 256), BF16),
             pltpu.VMEM((8, NZ, NY, 8, 256), BF16),
+            pltpu.VMEM((2, FAR, NY, 8, 256), BF16),
             pltpu.VMEM((8, 256), F32),
             pltpu.VMEM((NZ, 1, 128), F32),
             pltpu.VMEM((NZ, 1, 128), F32),
             pltpu.VMEM((NY, NZ, 1, 128), F32),
-            pltpu.VMEM((NY, 2, 128), F32),
-            pltpu.VMEM((NY, 2, 128), F32),
-            pltpu.VMEM((2, 128), F32),
-            pltpu.VMEM((NZ, 2, 128), F32),
-            pltpu.VMEM((2, 128), F32),
-            pltpu.VMEM((NY, 2, 128), F32),
+            pltpu.VMEM((8, 1, 128), F32),
+            pltpu.VMEM((8, 128), F32),
+            pltpu.VMEM((10, 8, 128), F32),
+            pltpu.VMEM((2, 8, 128), F32),
+            pltpu.VMEM((8, 128), F32),
+            pltpu.VMEM((NY, 8, 128), F32),
             pltpu.VMEM((2, 128), F32),
             pltpu.VMEM((8, 2, 128), F32),
             pltpu.VMEM((512, 256), BF16),
             dma((9,)),
-            regular((3,)),
-            dma, dma, dma, dma,
-            dma((9,)), dma((9,)), dma((9,)), dma((9,)), dma((9,)),
-            dma, dma, dma, dma,
+            regular((2,)),
+            dma, dma, dma, dma, dma, dma,
+            dma((9,)), dma((5,)), dma((9,)), dma((9,)),
+            dma, dma, dma, dma, dma, dma,
             dma((4,)), dma((4,)),
         ],
         compiler_params=pltpu.CompilerParams(

time: 47.2 us -> 43.4 us (0.919)
  Pallas kernels: 46.4 us -> 42.7 us
    pallas_call x1, Pallas kernels: 45.6 us -> 41.8 us  [body(): pl.pallas_call(kernel, out_shape=shapes, in_specs=[hbm] * 8, out_specs=(v...]
where the time goes in v3:
time: 43.4 us; the launch traced here: 43.3 us
  Pallas kernels  42.7 us (98%)
  between operations  0.64 us (1%)
    pallas_call x1, Pallas kernels, body(): pl.pallas_call(kernel, out_shape=shapes, in_specs=[hbm] * 8, out_specs=(v...  41.8 us

profile of v3, /device:TPU:1, one launch (start us, length us, event | category | flops | bytes accessed | tf_op | source)
XLA Modules:
  0.0 43.3 jit_solution(8269724317400418051)
XLA Ops:
  0.6 41.8 %shard_map.111 = (bf16[2,256,256]{2,1,0:T(8,128)(2,1)S(1)}, bf16[2,256,256]{2,1,0:T(8,128)(2,1)S(1)}, f32[2,4,256]{2,1,0:T(4,128)S(1)}, bf16[2,32]{1,0:T(2,128)(2,1)S(1)}) custom-call(bf16[2,256,2048]{2,1,0:T(8,128)(2,1)} %tok_hbm.1, bf16[2048,256]{1,0:T(8,128)(2,1)} %wk_hbm.1, bf16[2048,256]{1,0:T(8,128)(2,1)} %wv_hbm.1, f32[2,4,256]{2,1,0:T(4,128)} %bitcast.14, ...), custom_call_target="tpu_custom_call" | custom-call | tf_op jit(solution)/shard_map/pallas_call | solution.py:432
  42.5 0.8 %shard_map.112 = (bf16[2,256,256]{2,1,0:T(8,128)(2,1)}, bf16[2,256,256]{2,1,0:T(8,128)(2,1)}, f32[2,4,256]{2,1,0:T(4,128)}, bf16[2,32]{1,0:T(2,128)(2,1)}) custom-call(bf16[2,256,256]{2,1,0:T(8,128)(2,1)S(1)} %get-tuple-element.12.refs_0_, bf16[2,256,256]{2,1,0:T(8,128)(2,1)S(1)} %get-tuple-element.13.refs_1_, f32[2,4,256]{2,1,0:T(4,128)S(1)} %get-tuple-element.14.refs_2_, ...), custom_call_target="tpu_custom_call" | custom-call | tf_op jit(solution)/shard_map/pallas_call | solution.py:483

commit v4 on v3

--- a/solution.py
+++ b/solution.py
@@ -12,6 +12,7 @@
 NZ, NY, NX, NC = 16, 4, 4, 2
 HIGH = lax.Precision.HIGHEST
 FAR = 4
+KV_SLOT = 5
 
 
 def slots_of(d):
@@ -54,8 +55,8 @@
     tok_hbm, wk_hbm, wv_hbm, gate_hbm, new_in_hbm, query_hbm, new_gate_hbm, ow_hbm,
     k_out, v_out, g_out, m_out,
     tok, wk, wv, part, gate_ref, new_in_ref, query_ref, new_gate_ref, ow_ref,
-    order, sent, tbuf, relay, g8, pg, zg, yg, grelay, azs, az, far, afs, af, tps, tpr, kv_loc,
-    sem_in, d_sem, zs_sem, ys_sem, ls_sem, rs_sem, xs_sem, cs_sem, zr_sem, lr_sem, xr_sem, cr_sem,
+    order, sent, sent_kv, kv_in, tbuf, relay, g8, pg, zg, yg, grelay, azs, az, far, afs, af, tps, tpr, kv_loc,
+    sem_in, d_sem, zs_sem, ks_sem, ys_sem, ls_sem, rs_sem, xs_sem, cs_sem, zr_sem, lr_sem, xr_sem, cr_sem,
     gzs_sem, gzr_sem, grs_sem, grr_sem, gys_sem, gyr_sem, a_send, a_recv,
 ):
     z, y = lax.axis_index("z"), lax.axis_index("y")
@@ -118,6 +119,16 @@
                     z=to, y=yat(dy),
                 ).start()
 
+    def send_kv(d):
+        for sign in (1, -1):
+            to = zat(sign * d)
+            for dy in range(NY):
+                for q in range(2):
+                    remote(
+                        sent_kv.at[q, to, yat(dy)], kv_in.at[q, slot_at(d, sign) - KV_SLOT, y],
+                        ks_sem, zr_sem.at[d], z=to, y=yat(dy),
+                    ).start()
+
     def to_relay(k):
         for way, sign in enumerate((1, -1)):
             to = zat(sign * (FAR + k))
@@ -156,6 +167,29 @@
         for dx in range(1, NX):
             came = tbuf.at[xat(dx) * NC + c, slots(d)]
             remote(came, came, cs_sem, cr_sem.at[d], c=1 - c).start()
+
+    def lay_out(rows, out, first, count):
+        rows = rows.reshape(count * 2, 2, 8, 256)
+        even, odd = rows[:, 0], rows[:, 1]
+        low = iota(even.shape, 1) < 4
+        for b, (a0, a1) in enumerate(
+            ((even, pltpu.roll(odd, 4, 1)), (pltpu.roll(even, 4, 1), odd))
+        ):
+            block = jnp.where(low, a0, a1).reshape(count, 16, 256).astype(BF16)
+            for k in range(count):
+                slot = first + k
+                rel = 0 if slot == 0 else 8 if slot == NZ - 1 else (
+                    (slot + 1) // 2 if slot % 2 else -(slot // 2)
+                )
+                at = pl.multiple_of(zat(rel) * 16, 16)
+                out[b, pl.ds(at, 16), :] = block[k]
+
+    def place(d):
+        first, count = slots_of(d)
+        came = pl.ds(first - KV_SLOT, count)
+        wait_bytes(kv_in.at[:, came], zr_sem.at[d])
+        for q, out in enumerate((k_out, v_out)):
+            lay_out(kv_in[q, came].astype(F32), out, first, count)
 
     def finish(ds):
         for d in ds:
@@ -171,33 +205,22 @@
                     lhs, w[f * 256 : (f + 1) * 256, :], preferred_element_type=F32
                 )
                 acc = term if acc is None else acc + term
-            acc = acc.reshape(count * 2, 2, 8, 256)
-            even, odd = acc[:, 0], acc[:, 1]
-            low = iota(even.shape, 1) < 4
-            for b, (a0, a1) in enumerate(
-                ((even, pltpu.roll(odd, 4, 1)), (pltpu.roll(even, 4, 1), odd))
-            ):
-                block = jnp.where(low, a0, a1).reshape(count, 16, 256).astype(BF16)
-                for k in range(count):
-                    slot = first + k
-                    rel = 0 if slot == 0 else 8 if slot == NZ - 1 else (
-                        (slot + 1) // 2 if slot % 2 else -(slot // 2)
-                    )
-                    at = pl.multiple_of(zat(rel) * 16, 16)
-                    out[b, pl.ds(at, 16), :] = block[k]
+            lay_out(acc, out, first, count)
 
     pl.semaphore_wait(barrier, 3 + 7 + 8)
     for s in (1, -1):
         signal(d_sem.at[0], z=zat(s))
     load_part.wait()
-    for b in range(2):
-        for j in range(4):
-            for k in range(2):
-                order[k, pl.ds(4 * b + j, 64, stride=8), :] = part[
-                    b, 64 * j : 64 * j + 64, 128 * k : 128 * k + 128
-                ].astype(F32)
-    for k in range(2):
-        sent[:, :, :, 128 * k : 128 * k + 128] = order[k].reshape(NZ, NY, 8, 128).astype(BF16)
+    def rows_by_peer(rows, dst):
+        for k in range(2):
+            for b in range(2):
+                for j in range(4):
+                    order[k, pl.ds(4 * b + j, 64, stride=8), :] = rows(256 * b + 64 * j, k).astype(F32)
+            dst[:, :, :, 128 * k : 128 * k + 128] = order[k].reshape(NZ, NY, 8, 128).astype(BF16)
+
+    rows_by_peer(
+        lambda lo, k: part[lo // 256, lo % 256 : lo % 256 + 64, 128 * k : 128 * k + 128], sent
+    )
     for dy in range(1, NY):
         remote(
             sent.at[z, yat(dy)], tbuf.at[me, 0, y], ys_sem, zr_sem.at[0], y=yat(dy)
@@ -209,9 +232,6 @@
         signal(d_sem.at[1], z=zat(s))
     send_z(2)
 
-    pl.semaphore_wait(d_sem.at[1], 2)
-    to_relay(1)
-    to_relay(2)
     head_of_row = iota((8, 256), 0) & 3
     mine = (iota((8, 256), 1) >> 6) == head_of_row
     second = iota((8, 256), 0) >= 4
@@ -241,14 +261,17 @@
     for k in range(NZ):
         pg[k] = gate_rows[k : k + 1, :]
 
+    pl.semaphore_wait(d_sem.at[1], 2)
     to_relay(4)
+    to_relay(1)
+    to_relay(3)
     load_wk.wait()
     load_tok.wait()
     key_now = jnp.dot(new_in, wk[...], preferred_element_type=F32).astype(BF16).astype(F32)
     local = tok[...].reshape(512, 2048)
-    kv_loc[...] = jnp.dot(local, wk[...], preferred_element_type=F32).astype(BF16)
+    kv_loc[0] = jnp.dot(local, wk[...], preferred_element_type=F32).astype(BF16)
     raw = jnp.where(
-        second, nt_dot(query_b, kv_loc[256:, :]), nt_dot(query_b, kv_loc[:256, :])
+        second, nt_dot(query_b, kv_loc[0, 256:]), nt_dot(query_b, kv_loc[0, :256])
     )
     ng = new_gate_ref[...]
     ng = jnp.where(
@@ -264,16 +287,15 @@
     expo = jnp.exp(scores - top)
     total = jnp.sum(expo, axis=1, keepdims=True)
     expo_b = expo.astype(BF16)
-    x_first(1)
     x_first(0)
     load_wv.wait()
-    kv_loc[...] = jnp.dot(local, wv[...], preferred_element_type=F32).astype(BF16)
+    kv_loc[1] = jnp.dot(local, wv[...], preferred_element_type=F32).astype(BF16)
+    x_first(1)
     x_first(2)
-    send_z(3)
     num = jnp.where(
         second,
-        jnp.dot(expo_b, kv_loc[256:, :], preferred_element_type=F32),
-        jnp.dot(expo_b, kv_loc[:256, :], preferred_element_type=F32),
+        jnp.dot(expo_b, kv_loc[1, 256:], preferred_element_type=F32),
+        jnp.dot(expo_b, kv_loc[1, :256], preferred_element_type=F32),
     )
     num = fold_heads(jnp.where(mine, num, 0.0))
     lane = iota((8, 128), 1)
@@ -285,13 +307,6 @@
         for sign in (1, -1):
             slot = d - 1 if sign < 0 else FAR + d - 1
             remote(azs, az.at[slot], a_send.at[0], a_recv.at[0], z=zat(sign * d)).start()
-    to_relay(3)
-    x_second(0)
-    x_second(1)
-    pass_on(1)
-    send_z(4)
-    pass_on(2)
-    x_first(3)
     zg[z] = pg[z]
     for sign in (1, -1):
         for d in range(1, FAR + 1):
@@ -302,16 +317,21 @@
                 pg.at[zat(sign * (FAR + k))], grelay.at[FAR * way + k - 1], gzs_sem, grr_sem,
                 z=zat(sign * FAR),
             ).start()
+    to_relay(2)
+    pass_on(1)
+    x_second(0)
+    for q in range(2):
+        rows_by_peer(lambda lo, k: kv_loc[q, lo : lo + 64, 128 * k : 128 * k + 128], sent_kv.at[q])
+    pass_on(3)
+    pass_on(4)
+    x_second(1)
+    value_now = jnp.dot(new_in, wv[...], preferred_element_type=F32).astype(BF16).astype(F32)
     wait_bytes(az.at[pl.ds(0, 8)], a_recv.at[0])
     far[0] = merge([az[k] for k in range(FAR)])
     far[1] = merge([az[k] for k in range(FAR, 2 * FAR - 1)])
     remote(far.at[0], az.at[8], a_send.at[1], a_recv.at[1], z=zat(-FAR)).start()
     remote(far.at[1], az.at[9], a_send.at[1], a_recv.at[1], z=zat(FAR)).start()
-    pass_on(3)
-    x_first(5)
-    pass_on(4)
-    x_first(6)
-    x_first(4)
+    x_second(2)
     wait_bytes(zg.at[pl.ds(0, 7)], grr_sem)
     for way, sign in enumerate((1, -1)):
         for k in range(1, FAR + 1 - way):
@@ -319,19 +339,25 @@
                 grelay.at[FAR * way + k - 1], zg.at[zat(-sign * FAR)], grs_sem, gzr_sem,
                 z=zat(sign * k),
             ).start()
+    pass_on(2)
+    x_first(5)
+    x_first(7)
+    send_kv(4)
+    wait_bytes(zg.at[pl.ds(0, 15)], gzr_sem)
+    for dy in range(1, NY):
+        remote(zg, yg.at[y], gys_sem, gyr_sem, y=yat(dy)).start()
+    for k in range(NZ):
+        yg[y, k] = zg[k]
+    x_first(8)
     wait_bytes(az.at[pl.ds(8, 2)], a_recv.at[1])
     merged = merge([azs[...]] + [az[k] for k in range(10)])
     afs[...] = merged
     af[y] = merged
     for dy in range(1, NY):
         remote(afs, af.at[y], a_send.at[2], a_recv.at[2], y=yat(dy)).start()
-    x_first(7)
-    x_first(8)
-    x_second(2)
-    x_second(3)
-    value_now = jnp.dot(new_in, wv[...], preferred_element_type=F32).astype(BF16).astype(F32)
-    x_second(5)
-    x_second(6)
+    send_kv(3)
+    x_first(6)
+    x_second(7)
     load_ow.wait()
     wait_bytes(af.at[pl.ds(0, 3)], a_recv.at[2])
     cached = merge([af[k] for k in range(NY)])
@@ -361,21 +387,7 @@
                     tps, tpr.at[me], a_send.at[3], a_recv.at[3],
                     x=xat(dx), c=lax.rem(c + dc, NC),
                 ).start()
-    x_second(4)
-    wait_bytes(zg.at[pl.ds(0, 15)], gzr_sem)
-    for dy in range(1, NY):
-        remote(zg, yg.at[y], gys_sem, gyr_sem, y=yat(dy)).start()
-    for k in range(NZ):
-        yg[y, k] = zg[k]
-    finish((5, 6))
-    finish((0, 1, 2, 3, 4))
-    x_second(7)
     x_second(8)
-    wait_bytes(tpr.at[pl.ds(0, 7)], a_recv.at[3])
-    mixed = tpr[0]
-    for k in range(1, NX * NC):
-        mixed += tpr[k]
-    m_out[...] = mixed[:, :32].astype(BF16)
     wait_bytes(yg.at[pl.ds(0, 3)], gyr_sem)
     field = (iota((16, 128), 1) >> 2) & 3
     gathered = jnp.zeros((16, 128), F32)
@@ -392,13 +404,25 @@
     gate_cols = nt_dot(pick.astype(F32), spread, HIGH)
     g_out[0] = gate_cols[0:4]
     g_out[1] = gate_cols[4:8]
+    x_second(5)
+    x_second(6)
+    finish((0, 1, 2))
+    place(4)
     finish((7, 8))
-    wait_bytes(sent.at[pl.ds(0, 8)], zs_sem)
+    place(3)
+    finish((5, 6))
+    wait_bytes(tpr.at[pl.ds(0, 7)], a_recv.at[3])
+    mixed = tpr[0]
+    for k in range(1, NX * NC):
+        mixed += tpr[k]
+    m_out[...] = mixed[:, :32].astype(BF16)
+    wait_bytes(sent.at[pl.ds(0, 4)], zs_sem)
+    wait_bytes(sent.at[pl.ds(0, 8)], ks_sem)
     wait_bytes(tbuf.at[0, 0, pl.ds(0, 3)], ys_sem)
     wait_bytes(sent.at[pl.ds(0, 7)], ls_sem)
     wait_bytes(sent.at[pl.ds(0, 7)], rs_sem)
-    wait_bytes(tbuf.at[pl.ds(0, 3)], xs_sem)
-    wait_bytes(tbuf.at[pl.ds(0, 4)], cs_sem)
+    wait_bytes(tbuf.at[pl.ds(0, 3), pl.ds(0, 12)], xs_sem)
+    wait_bytes(tbuf.at[pl.ds(0, 4), pl.ds(0, 12)], cs_sem)
     wait_bytes(zg.at[pl.ds(0, 15)], gzs_sem)
     wait_bytes(zg.at[pl.ds(0, 7)], grs_sem)
     wait_bytes(yg.at[pl.ds(0, 3)], gys_sem)
@@ -446,6 +470,8 @@
             pltpu.VMEM((32, 256), BF16),
             pltpu.VMEM((2, 512, 128), F32),
             pltpu.VMEM((NZ, NY, 8, 256), BF16),
+            pltpu.VMEM((2, NZ, NY, 8, 256), BF16),
+            pltpu.VMEM((2, 4, NY, 8, 256), BF16),
             pltpu.VMEM((8, NZ, NY, 8, 256), BF16),
             pltpu.VMEM((2, FAR, NY, 8, 256), BF16),
             pltpu.VMEM((8, 256), F32),
@@ -460,10 +486,10 @@
             pltpu.VMEM((NY, 8, 128), F32),
             pltpu.VMEM((2, 128), F32),
             pltpu.VMEM((8, 2, 128), F32),
-            pltpu.VMEM((512, 256), BF16),
+            pltpu.VMEM((2, 512, 256), BF16),
             dma((9,)),
             regular((2,)),
-            dma, dma, dma, dma, dma, dma,
+            dma, dma, dma, dma, dma, dma, dma,
             dma((9,)), dma((5,)), dma((9,)), dma((9,)),
             dma, dma, dma, dma, dma, dma,
             dma((4,)), dma((4,)),

time: 43.4 us -> 42.8 us (0.986)
  Pallas kernels: 42.7 us -> 42.1 us
    pallas_call x1, Pallas kernels: 41.8 us -> 41.2 us  [body(): pl.pallas_call(kernel, out_shape=shapes, in_specs=[hbm] * 8, out_specs=(v...]
where the time goes in v4:
time: 42.8 us; the launch traced here: 42.7 us
  Pallas kernels  42.1 us (98%)
  between operations  0.64 us (1%)
    pallas_call x1, Pallas kernels, body(): pl.pallas_call(kernel, out_shape=shapes, in_specs=[hbm] * 8, out_specs=(v...  41.2 us

profile of v4, /device:TPU:1, one launch (start us, length us, event | category | flops | bytes accessed | tf_op | source)
XLA Modules:
  0.0 42.7 jit_solution(15219056199716087641)
XLA Ops:
  0.6 41.2 %shard_map.111 = (bf16[2,256,256]{2,1,0:T(8,128)(2,1)S(1)}, bf16[2,256,256]{2,1,0:T(8,128)(2,1)S(1)}, f32[2,4,256]{2,1,0:T(4,128)S(1)}, bf16[2,32]{1,0:T(2,128)(2,1)S(1)}) custom-call(bf16[2,256,2048]{2,1,0:T(8,128)(2,1)} %tok_hbm.1, bf16[2048,256]{1,0:T(8,128)(2,1)} %wk_hbm.1, bf16[2048,256]{1,0:T(8,128)(2,1)} %wv_hbm.1, f32[2,4,256]{2,1,0:T(4,128)} %bitcast.14, ...), custom_call_target="tpu_custom_call" | custom-call | tf_op jit(solution)/shard_map/pallas_call | solution.py:456
  41.9 0.8 %shard_map.112 = (bf16[2,256,256]{2,1,0:T(8,128)(2,1)}, bf16[2,256,256]{2,1,0:T(8,128)(2,1)}, f32[2,4,256]{2,1,0:T(4,128)}, bf16[2,32]{1,0:T(2,128)(2,1)}) custom-call(bf16[2,256,256]{2,1,0:T(8,128)(2,1)S(1)} %get-tuple-element.12.refs_0_, bf16[2,256,256]{2,1,0:T(8,128)(2,1)S(1)} %get-tuple-element.13.refs_1_, f32[2,4,256]{2,1,0:T(4,128)S(1)} %get-tuple-element.14.refs_2_, ...), custom_call_target="tpu_custom_call" | custom-call | tf_op jit(solution)/shard_map/pallas_call | solution.py:509
